TPU v7x, 256 devices: a whole 4x4x8 slice. The times are simulated.
256 devices in a mesh: ep: 64 (over z, y, core), tp: 4 (over x).
Axes of the slice: x: 4, y: 4, z: 8, core: 2. Of those that a mesh axis runs over, the one named last changes fastest.
Arguments:
- tokens: bfloat16 [16384, 1024], P('ep'), may hold values from -6 to 6
- cotangent: bfloat16 [16384, 1024], P('ep'), may hold values from -1.5 to 1.5
- routing: int32 [16384, 2], P('ep'), may hold values from 0 to 127, all different within a row; in each aligned block of 256 rows (0 to 255, 256 to 511, ...) at most 12 rows name the same one
- gate_weights: float32 [16384, 2], P('ep'), may hold values from 0.1 to 0.9
- gate_proj: bfloat16 [128, 1024, 512], P('ep', None, 'tp'), may hold values from -0.1875 to 0.1875
- up_proj: bfloat16 [128, 1024, 512], P('ep', None, 'tp'), may hold values from -0.1875 to 0.1875
- down_proj: bfloat16 [128, 512, 1024], P('ep', 'tp'), may hold values from -0.25 to 0.25
Outputs:
- tokens_grad: bfloat16 [16384, 1024], P('ep')
- gates_grad: float32 [16384, 2], P('ep')
- gate_proj_grad: float32 [128, 1024, 512], P('ep', None, 'tp')
- up_proj_grad: float32 [128, 1024, 512], P('ep', None, 'tp')
- down_proj_grad: float32 [128, 512, 1024], P('ep', 'tp')
Inputs may be any that keep to these rules, and one draw needn't show every extreme that they name: `routing`: each row names 2 different experts; every expert is named by some row; within each aligned block of 256 rows (the tokens of one index of ep) no expert is named by more than 12 rows, a bound that some block reaches.
All inputs are finite; a program needn't handle non-finite values.
Results may differ from a plain program's by a relative error of at most 0.0015.
Values may be sent and summed in bfloat16 or wider, within the bound.
A program may use at most 128 MiB of HBM per device.

v0:
```python
import jax
import jax.numpy as jnp
from jax import lax
from jax.experimental import pallas as pl
from jax.experimental.pallas import tpu as pltpu
from jax.sharding import PartitionSpec as P

F32 = jnp.float32
BF16 = jnp.bfloat16
I32 = jnp.int32
MESH = pl.DeviceIdType.MESH

NZ, NY, NC, NX = 8, 4, 2, 4
PLANE = NY * NC
TOK = 256
D = 1024
Q = 256
FS = 128
CAP = 12
SLOT = 2 * CAP
ROWS = PLANE * SLOT
ALL = NZ * ROWS
DENSE = TOK + 8
POS = {0: 0, 1: 1, 7: 2, 2: 3, 6: 4, 3: 5, 5: 6, 4: 7}
PARTS = ((0, 128), (128, DENSE - 128))
CONTRACT_MINOR = (((1,), (1,)), ((), ()))
CONTRACT_MAJOR = (((0,), (0,)), ((), ()))


def kernel(
    tok, cot, rt, gw, wg, wu, wd,
    tg_out, gg_out, dg_out, du_out, dd_out,
    bk, rb, other, sx, so, rx, xl, xr, wv, wgu, wds, wq, sl, upper, pk, wt, ts, gu2, h2,
    gx, pr, prx, prs, prr, igs, igr, db, rm, rp, tq, dg, du, dd,
    in_s, z_s, z_r, rb_s, rb_r, ip_s, ip_r, io_s, io_r, x_s, x_r, w_s, w_r, g_s, g_r, gf_s, gf_r,
    p_s, p_r, pp_s, pp_r, ig_s, ig_r, c_s, c_r, t_s, t_r, out_s,
):
    e = lax.axis_index("ep")
    x = lax.axis_index("tp")
    z = e // PLANE
    y = (e % PLANE) // NC
    c = e % NC
    half = x % 2

    def at_z(step):
        return (((z + step) % NZ) * PLANE + y * NC + c, x)

    def at_plane(j, sign):
        dy, dc = j // NC, j % NC
        return (z * PLANE + ((y + sign * dy + NY) % NY) * NC + (c + dc) % NC, x)

    def at_x(step):
        return (e, (x + step) % NX)

    def remote(src, dst, ssem, rsem, dev):
        return pltpu.make_async_remote_copy(
            src_ref=src, dst_ref=dst, send_sem=ssem, recv_sem=rsem,
            device_id=dev, device_id_type=MESH,
        )

    def done(ref, sem):
        pltpu.make_async_copy(ref, ref, sem).wait()

    sends = []

    def push(src, dst, ssem, rsem, dev, last=True):
        remote(src, dst, ssem, rsem, dev).start()
        if last:
            sends.append((src, ssem))

    def quarter(k):
        return 2 * half + k if k < 2 else 2 * (1 - half) + (k - 2)

    with jax.named_scope("prologue"):
        barrier = pltpu.get_barrier_semaphore()
        partners = [at_z(1), at_z(NZ - 1)]
        partners += [at_plane(j, 1) for j in range(1, PLANE)]
        partners += [at_x(s) for s in range(1, NX)]
        for dev in partners:
            pl.semaphore_signal(barrier, inc=1, device_id=dev, device_id_type=MESH)

        loads = []
        for k in range(4):
            cols = pl.ds(pl.multiple_of(quarter(k) * Q, Q), Q)
            dst = bk.at[0, k] if k < 2 else other.at[k - 2]
            loads.append(pltpu.make_async_copy(tok.at[:, cols], dst.at[0], in_s.at[2 * k]))
            loads.append(pltpu.make_async_copy(cot.at[:, cols], dst.at[1], in_s.at[2 * k + 1]))
        for i, w in enumerate((wg, wu)):
            loads.append(pltpu.make_async_copy(w, wv.at[i], in_s.at[8 + i]))
        for q in range(4):
            for i in range(2):
                loads.append(
                    pltpu.make_async_copy(
                        wd.at[i, :, pl.ds(q * Q, Q)], wds.at[q, pl.ds(i * FS, FS)], in_s.at[10 + 2 * q + i]
                    )
                )
        for load in loads:
            load.start()
        rb[0] = jnp.concatenate(
            [rt[...].astype(F32), gw[...], jnp.zeros((4, TOK), F32)], axis=0
        )
        upper[...] = (
            lax.broadcasted_iota(I32, (TOK, TOK), 0) < lax.broadcasted_iota(I32, (TOK, TOK), 1)
        ).astype(F32).astype(BF16)
        for load in loads[:4]:
            load.wait()
    with jax.named_scope("barrier"):
        pl.semaphore_wait(barrier, len(partners))

    def first_of(n, lanes):
        i = lax.broadcasted_iota(I32, (n * PLANE, SLOT, lanes), 1)
        return (i < CAP).reshape(n * ROWS, lanes)

    def lane_of_slot(n):
        i = lax.broadcasted_iota(I32, (n * PLANE, SLOT, FS), 1)
        l = lax.broadcasted_iota(I32, (n * PLANE, SLOT, FS), 2)
        return i == l

    def z_push(dz, h, plus):
        if plus:
            to, dev, i = dz + 1, at_z(1), h
        else:
            to, dev, i = (dz + NZ - 1) % NZ, at_z(NZ - 1), 2 + h
        push(bk.at[dz, h], bk.at[to, h], z_s.at[i, dz], z_r.at[h, to], dev)

    def rb_push(dz, plus):
        if plus:
            to, dev, i = dz + 1, at_z(1), 0
        else:
            to, dev, i = (dz + NZ - 1) % NZ, at_z(NZ - 1), 1
        push(rb.at[dz], rb.at[to], rb_s.at[i, dz], rb_r.at[to], dev)

    @jax.named_scope("slots_of")
    def slots_of(dz):
        pos = POS[dz]
        e16 = lax.broadcasted_iota(I32, (16, TOK), 0)
        target = ((e16 // 4 - y) & 3) * NC + (((e16 // 2) - c) & 1)
        base = (target * SLOT + (e16 & 1) * CAP).astype(F32)
        block = rb[dz]
        chosen = block[0:2].astype(I32) - z * 16
        e0 = (e16 == chosen[0:1]).astype(F32)
        e1 = (e16 == chosen[1:2]).astype(F32)
        both = jnp.concatenate([e0, e1], axis=0).astype(BF16)
        before = jnp.dot(both, upper[...], preferred_element_type=F32)
        before0 = before[0:16]
        before1 = before[16:32] + jnp.sum(e0, axis=1, keepdims=True)
        s0 = jnp.sum(e0 * (base + before0 + 1.0), axis=0, keepdims=True) - 1.0
        s1 = jnp.sum(e1 * (base + before1 + 1.0), axis=0, keepdims=True) - 1.0
        slots = jnp.concatenate([s0, s1], axis=0).astype(I32)
        sl[pos, 0:2] = slots
        row = lax.broadcasted_iota(I32, (ROWS, TOK), 0)
        p0 = row == slots[0:1]
        p1 = row == slots[1:2]
        pk[pos] = (p0 | p1).astype(F32).astype(BF16)
        weight = jnp.sum(
            jnp.where(p0, block[2:3], 0.0) + jnp.where(p1, block[3:4], 0.0),
            axis=1, keepdims=True,
        )
        wt[pos] = jnp.broadcast_to(weight, (ROWS, FS))

    @jax.named_scope("build")
    def build(dz, h, src, stage, land, ssem, rsem):
        pos = POS[dz]
        pick = pk[pos]
        w = jnp.concatenate([wt[pos], wt[pos]], axis=1)
        t = jnp.dot(pick, src[0], preferred_element_type=F32)
        s = jnp.dot(pick, src[1], preferred_element_type=F32) * w
        t = t.reshape(PLANE, 3, 8, Q).astype(BF16)
        s = s.reshape(PLANE, 3, 8, Q).astype(BF16)
        stage[:, 0:3] = t
        stage[:, 3:6] = s
        land[0, 0:3] = t[0]
        land[0, 3:6] = s[0]
        for j in range(1, PLANE):
            push(stage.at[j], land.at[j], ssem, rsem, at_plane(j, 1), last=False)
        sends.append((stage.at[pl.ds(1, PLANE - 1)], ssem))

    def build_half(dz, h):
        pos = POS[dz]
        build(dz, h, bk.at[dz, h], sx.at[pos, h], rx.at[h, pos], ip_s.at[h, pos], ip_r.at[h, pos])

    @jax.named_scope("x_push")
    def x_push(dz, h):
        pos = POS[dz]
        done(rx.at[h, pos, pl.ds(1, PLANE - 1)], ip_r.at[h, pos])
        dst = xl if h == 0 else xr
        push(rx.at[h, pos], dst.at[pos], x_s.at[h, pos], x_r.at[h, pos], at_x(1 if h == 0 else NX - 1))

    @jax.named_scope("compute_wait")
    def compute_wait(p, n):
        for i in range(p, p + n):
            if i == 0:
                for h in range(2):
                    done(rx.at[h, 0, pl.ds(1, PLANE - 1)], ip_r.at[h, 0])
                done(xl.at[0, pl.ds(1, PLANE - 1)], io_r.at[0])
                done(xr.at[0, pl.ds(1, PLANE - 1)], io_r.at[1])
            else:
                done(xl.at[i], x_r.at[0, i])
                done(xr.at[i], x_r.at[1, i])

    @jax.named_scope("compute")
    def compute(p, n):
        m = n * ROWS
        rows = pl.ds(p * ROWS, m)
        pre = jnp.zeros((m, 512), F32)
        hg = jnp.zeros((m, 256), F32)
        for k, src in enumerate((rx.at[0], rx.at[1], xl, xr)):
            t = src[p:p + n, :, 0:3].astype(F32).reshape(m, Q).astype(BF16)
            s = src[p:p + n, :, 3:6].astype(F32).reshape(m, Q).astype(BF16)
            ts[k, 0, rows] = t
            ts[k, 1, rows] = s
            pre = pre + jnp.dot(t, wgu[quarter(k)], preferred_element_type=F32)
            hg = hg + lax.dot_general(
                s, wds[quarter(k)], CONTRACT_MINOR, preferred_element_type=F32
            )
        first = first_of(n, FS)
        g = jnp.where(first, pre[:, 0:128], pre[:, 128:256]).astype(BF16).astype(F32)
        u = jnp.where(first, pre[:, 256:384], pre[:, 384:512]).astype(BF16).astype(F32)
        dh = jnp.where(first, hg[:, 0:128], hg[:, 128:256])
        sg = jax.nn.sigmoid(g)
        act = g * sg
        hidden = act * u
        product = jnp.sum(dh * hidden, axis=1, keepdims=True)
        placed = jnp.where(
            lane_of_slot(n),
            jnp.broadcast_to(product, (m, FS)).reshape(n * PLANE, SLOT, FS),
            0.0,
        )
        pr[p:p + n] = jnp.sum(placed, axis=1).reshape(n, PLANE, FS)
        gg = dh * u * sg * (1.0 + g * (1.0 - sg))
        ug = dh * act
        gx[0, rows, 0:FS] = gg.astype(BF16)
        gx[0, rows, FS:2 * FS] = ug.astype(BF16)
        for i, v in enumerate((gg, ug, hidden)):
            lo = jnp.where(first, v, 0.0).astype(BF16)
            hi = jnp.where(first, 0.0, v).astype(BF16)
            if i < 2:
                gu2[rows, 256 * i:256 * i + 128] = lo
                gu2[rows, 256 * i + 128:256 * i + 256] = hi
            else:
                h2[rows, 0:128] = lo
                h2[rows, 128:256] = hi

    @jax.named_scope("weight_grads")
    def weight_grads(k):
        at = pl.ds(pl.multiple_of(quarter(k) * Q, Q), Q)
        o = lax.dot_general(ts[k, 0], gu2[...], CONTRACT_MAJOR, preferred_element_type=F32)
        for i in range(2):
            dg[i, at, :] = o[:, i * FS:(i + 1) * FS]
            du[i, at, :] = o[:, 256 + i * FS:256 + (i + 1) * FS]
        o = lax.dot_general(h2[...], ts[k, 1], CONTRACT_MAJOR, preferred_element_type=F32)
        for i in range(2):
            dd[i, :, at] = o[i * FS:(i + 1) * FS]

    def rows_of(dz, lo=0, n=ROWS):
        return pl.ds(POS[dz] * ROWS + lo, n)

    def g_push(dz):
        r = rows_of(dz)
        push(gx.at[0, r], gx.at[1, r], g_s.at[0, dz], g_r.at[0, dz], at_x(1))
        push(gx.at[0, r], gx.at[2, r], g_s.at[1, dz], g_r.at[1, dz], at_x(NX - 1))

    @jax.named_scope("g_pass")
    def g_pass(dz):
        lo, hi = rows_of(dz, 0, 96), rows_of(dz, 96, 96)
        done(gx.at[1, rows_of(dz)], g_r.at[0, dz])
        push(gx.at[1, lo], gx.at[3, lo], gf_s.at[0, dz], gf_r.at[0, dz], at_x(1))
        done(gx.at[2, rows_of(dz)], g_r.at[1, dz])
        push(gx.at[2, hi], gx.at[3, hi], gf_s.at[1, dz], gf_r.at[1, dz], at_x(NX - 1))

    @jax.named_scope("ig_wait")
    def ig_wait(dz):
        done(gx.at[3, rows_of(dz, 0, 96)], gf_r.at[0, dz])
        done(gx.at[3, rows_of(dz, 96, 96)], gf_r.at[1, dz])

    @jax.named_scope("input_grad")
    def input_grad(dz):
        pos = POS[dz]
        first = first_of(1, FS)
        total = jnp.zeros((ROWS, Q), F32)
        for slot, w in ((0, None), (1, 0), (2, 2), (3, 1)):
            pair = gx[slot, rows_of(dz)].astype(F32)
            gg, ug = pair[:, 0:FS], pair[:, FS:2 * FS]
            lhs = jnp.concatenate(
                [
                    jnp.where(first, gg, 0.0).astype(BF16),
                    jnp.where(first, 0.0, gg).astype(BF16),
                    jnp.where(first, ug, 0.0).astype(BF16),
                    jnp.where(first, 0.0, ug).astype(BF16),
                ],
                axis=1,
            )
            rhs = wgu[x] if w is None else wq[w]
            total = total + lax.dot_general(lhs, rhs, CONTRACT_MINOR, preferred_element_type=F32)
        igs[pos] = total
        igr[pos, 0:SLOT] = total[0:SLOT]
        for j in range(1, PLANE):
            at = pl.ds(j * SLOT, SLOT)
            push(
                igs.at[pos, at], igr.at[pos, at], ig_s.at[pos], ig_r.at[pos], at_plane(j, -1),
                last=False,
            )
        sends.append((igs.at[pos, pl.ds(SLOT, ROWS - SLOT)], ig_s.at[pos]))

    @jax.named_scope("dense")
    def dense(dz):
        pos = POS[dz]
        with jax.named_scope("dense_wait"):
            done(igr.at[pos, pl.ds(SLOT, ROWS - SLOT)], ig_r.at[pos])
        pick = pk[pos]
        v = igr[pos]
        hi = v.astype(BF16)
        rest = v - hi.astype(F32)
        mid = rest.astype(BF16)
        low = (rest - mid.astype(F32)).astype(BF16)
        total = lax.dot_general(pick, hi, CONTRACT_MAJOR, preferred_element_type=F32)
        total = total + (
            lax.dot_general(pick, mid, CONTRACT_MAJOR, preferred_element_type=F32)
            + lax.dot_general(pick, low, CONTRACT_MAJOR, preferred_element_type=F32)
        )
        db[dz, 0:TOK] = total
        row = lax.broadcasted_iota(I32, (ROWS, TOK), 0)
        slots = sl[pos, 0:2]
        spread = jnp.broadcast_to(prr[:, pos][:, None, :], (PLANE, SLOT, FS))
        col = jnp.sum(
            jnp.where(lane_of_slot(1), spread, 0.0).reshape(ROWS, FS), axis=1, keepdims=True
        )
        r0 = jnp.sum(jnp.where(row == slots[0:1], col, 0.0), axis=0, keepdims=True)
        r1 = jnp.sum(jnp.where(row == slots[1:2], col, 0.0), axis=0, keepdims=True)
        db[dz, TOK:DENSE] = jnp.concatenate([r0, r1, jnp.zeros((6, Q), F32)], axis=0)

    def part(i):
        return pl.ds(*PARTS[i])

    @jax.named_scope("chain")
    def chain(dz):
        if dz == 4:
            push(db.at[4, part(0)], rm.at[3, part(0)], c_s.at[0, 4], c_r.at[0, 3], at_z(NZ - 1))
            push(db.at[4, part(1)], rp.at[0, part(1)], c_s.at[1, 4], c_r.at[1, 4], at_z(1))
        elif dz < 4:
            for i in (1, 0):
                if dz < 3 or i == 0:
                    done(rm.at[dz, part(i)], c_r.at[i, dz])
                    db[dz, part(i)] += rm[dz, part(i)]
                push(
                    db.at[dz, part(i)], rm.at[dz - 1, part(i)], c_s.at[i, dz], c_r.at[i, dz - 1],
                    at_z(NZ - 1),
                )
        else:
            for i in (0, 1):
                if dz > 5 or i == 1:
                    done(rp.at[dz - 5, part(i)], c_r.at[i, dz - 1])
                    db[dz, part(i)] += rp[dz - 5, part(i)]
                push(
                    db.at[dz, part(i)], rp.at[dz - 4, part(i)], c_s.at[i, dz], c_r.at[i, dz],
                    at_z(1),
                )

    for h in range(2):
        z_push(0, h, True)
        z_push(0, 1 - h, False)
        if h == 0:
            rb_push(0, True)
            rb_push(0, False)
    slots_of(0)
    for h in range(2):
        build_half(0, h)
    for load in loads[4:10]:
        load.wait()
    for h in range(2):
        build(
            0, h, other.at[h], so.at[h], (xl if h == 0 else xr).at[0], io_s.at[h], io_r.at[h]
        )
    with jax.named_scope("weights"):
        for q in range(4):
            for w in range(2):
                for i in range(2):
                    lane = 256 * w + FS * i
                    wgu[q, :, lane:lane + FS] = wv[w, i, q * Q:(q + 1) * Q, :]
        for s in range(1, NX):
            push(wgu.at[(x + s) % NX], wq.at[s - 1], w_s.at[s - 1], w_r.at[s - 1], at_x(s))
        for load in loads[10:]:
            load.wait()

    def arrivals(s):
        k = (s + 1) // 2
        if s == 7:
            return ((4, 0), (4, 1))
        return ((k, 0), (NZ - k, 1)) if s % 2 else ((k, 1), (NZ - k, 0))

    for s in range(1, 8):
        here = arrivals(s)
        with jax.named_scope("z_wait"):
            for i, (dz, h) in enumerate(here):
                if s % 2 and not (s == 7 and i == 1):
                    done(rb.at[dz], rb_r.at[dz])
                    if s == 7:
                        pass
                    elif i == 0:
                        rb_push(dz, True)
                    elif s < 5:
                        rb_push(dz, False)
                done(bk.at[dz, h], z_r.at[h, dz])
                if s < 6:
                    z_push(dz, h, i == 0)
        if s % 2:
            for dz in dict.fromkeys(dz for dz, _ in here):
                slots_of(dz)
        for dz, h in here:
            build_half(dz, h)
        if s > 1:
            for dz, h in arrivals(s - 1):
                x_push(dz, h)
        if s == 2:
            compute_wait(0, 1)
            compute(0, 1)
            g_push(0)
        if s == 4:
            g_pass(0)
            compute_wait(1, 2)
            compute(1, 2)
        if s == 6:
            compute_wait(3, 2)
            compute(3, 2)
        if s == 5:
            with jax.named_scope("wq_wait"):
                for i in range(NX - 1):
                    done(wq.at[i], w_r.at[i])
            ig_wait(0)
            input_grad(0)
    for dz, h in arrivals(7):
        x_push(dz, h)
    compute_wait(5, 2)
    compute(5, 2)
    compute_wait(7, 1)
    compute(7, 1)

    back = (4, 3, 5, 2, 6, 1, 7)
    for dz in back[:3]:
        g_push(dz)
    for s in range(1, NX):
        push(pr, prx.at[s - 1], p_s.at[s - 1], p_r.at[s - 1], at_x(s))
    weight_grads(0)

    def products():
        with jax.named_scope("products"):
            for s in range(NX - 1):
                done(prx.at[s], p_r.at[s])
            total = pr[...] + prx[0] + prx[1] + prx[2]
            for j in range(PLANE):
                prs[j] = total[:, j]
            prr[0] = total[:, 0]
            for j in range(1, PLANE):
                push(prs.at[j], prr.at[j], pp_s, pp_r, at_plane(j, -1), last=False)
            sends.append((prs.at[pl.ds(1, PLANE - 1)], pp_s))

    outs = []

    def put(src, dst, sem):
        copy = pltpu.make_async_copy(src, dst, sem)
        copy.start()
        outs.append(copy)

    chains = {2: (4,), 4: (3, 5), 6: (2,), 7: (6,)}
    for i in range(8):
        if i < 7:
            g_pass(back[i])
            if i + 3 < 7:
                g_push(back[i + 3])
        if i == 0:
            products()
        if 1 <= i <= 7:
            ig_wait(back[i - 1])
            input_grad(back[i - 1])
        if i in (1, 2, 3):
            weight_grads(i)
        if i == 1:
            with jax.named_scope("products_wait"):
                done(prr.at[pl.ds(1, PLANE - 1)], pp_r)
        if i == 3:
            put(dg, dg_out, out_s.at[0])
            put(du, du_out, out_s.at[1])
            put(dd, dd_out, out_s.at[2])
        if i >= 2:
            dense(back[i - 2])
        if i == 3:
            dense(0)
        for dz in chains.get(i, ()):
            chain(dz)
    dense(7)
    chain(1)
    chain(7)

    t_rows = (pl.ds(0, 128), pl.ds(128, 128))
    with jax.named_scope("final"):
        for i in (0, 1):
            done(rm.at[0, part(i)], c_r.at[i, 0])
            done(rp.at[3, part(i)], c_r.at[i, 7])
            full = db[0, part(i)] + (rm[0, part(i)] + rp[3, part(i)])
            tq[0, t_rows[i]] = full[0:128].astype(BF16)
            push(tq.at[0, t_rows[i]], tq.at[1, t_rows[i]], t_s.at[0, i], t_r.at[0, i], at_x(1))
            push(tq.at[0, t_rows[i]], tq.at[2, t_rows[i]], t_s.at[1, i], t_r.at[1, i], at_x(NX - 1))
            if i == 1:
                gg_out[...] = full[128:130] / gw[...]

    def place(slot, who, sem):
        put(tq.at[slot], tg_out.at[:, pl.ds(pl.multiple_of(who * Q, Q), Q)], sem)

    with jax.named_scope("gather"):
        place(0, x, out_s.at[3])
        done(tq.at[1, t_rows[0]], t_r.at[0, 0])
        push(tq.at[1, t_rows[0]], tq.at[3, t_rows[0]], t_s.at[2, 0], t_r.at[2, 0], at_x(1))
        done(tq.at[2, t_rows[0]], t_r.at[1, 0])
        done(tq.at[2, t_rows[1]], t_r.at[1, 1])
        push(tq.at[2, t_rows[1]], tq.at[3, t_rows[1]], t_s.at[2, 1], t_r.at[2, 1], at_x(NX - 1))
        done(tq.at[1, t_rows[1]], t_r.at[0, 1])
        place(1, (x + NX - 1) % NX, out_s.at[4])
        place(2, (x + 1) % NX, out_s.at[5])
    with jax.named_scope("drain"):
        for src, sem in sends:
            done(src, sem)
        for i in range(2):
            done(tq.at[3, t_rows[i]], t_r.at[2, i])
        place(3, (x + 2) % NX, out_s.at[6])
        for copy in outs:
            copy.wait()


def shards(tokens, cotangent, routing, gate_weights, gate_proj, up_proj, down_proj):
    vmem = pl.BlockSpec(memory_space=pltpu.VMEM)
    hbm = pl.BlockSpec(memory_space=pl.ANY)
    dma = pltpu.SemaphoreType.DMA
    scratch = [
        pltpu.VMEM((NZ, 2, 2, TOK, Q), BF16),
        pltpu.VMEM((NZ, 8, TOK), F32),
        pltpu.VMEM((2, 2, TOK, Q), BF16),
        pltpu.VMEM((NZ, 2, PLANE, 6, 8, Q), BF16),
        pltpu.VMEM((2, PLANE, 6, 8, Q), BF16),
        pltpu.VMEM((2, NZ, PLANE, 6, 8, Q), BF16),
        pltpu.VMEM((NZ, PLANE, 6, 8, Q), BF16),
        pltpu.VMEM((NZ, PLANE, 6, 8, Q), BF16),
        pltpu.VMEM((2, 2, D, FS), BF16),
        pltpu.VMEM((4, Q, 512), BF16),
        pltpu.VMEM((4, 256, Q), BF16),
        pltpu.VMEM((3, Q, 512), BF16),
        pltpu.VMEM((NZ, 8, TOK), I32),
        pltpu.VMEM((TOK, TOK), BF16),
        pltpu.VMEM((NZ, ROWS, TOK), BF16),
        pltpu.VMEM((NZ, ROWS, FS), F32),
        pltpu.VMEM((4, 2, ALL, Q), BF16),
        pltpu.VMEM((ALL, 512), BF16),
        pltpu.VMEM((ALL, 256), BF16),
        pltpu.VMEM((4, ALL, 256), BF16),
        pltpu.VMEM((NZ, PLANE, FS), F32),
        pltpu.VMEM((3, NZ, PLANE, FS), F32),
        pltpu.VMEM((PLANE, NZ, FS), F32),
        pltpu.VMEM((PLANE, NZ, FS), F32),
        pltpu.VMEM((NZ, ROWS, Q), F32),
        pltpu.VMEM((NZ, ROWS, Q), F32),
        pltpu.VMEM((NZ, DENSE, Q), F32),
        pltpu.VMEM((4, DENSE, Q), F32),
        pltpu.VMEM((4, DENSE, Q), F32),
        pltpu.VMEM((4, TOK, Q), BF16),
        pltpu.VMEM((2, D, FS), F32),
        pltpu.VMEM((2, D, FS), F32),
        pltpu.VMEM((2, FS, D), F32),
        dma((18,)), dma((4, 8)), dma((2, 8)), dma((2, 8)), dma((8,)),
        dma((2, 8)), dma((2, 8)), dma((2,)), dma((2,)), dma((2, 8)), dma((2, 8)),
        dma((3,)), dma((3,)), dma((2, 8)), dma((2, 8)), dma((2, 8)), dma((2, 8)),
        dma((3,)), dma((3,)), dma, dma, dma((8,)), dma((8,)),
        dma((2, 8)), dma((2, 8)), dma((3, 2)), dma((3, 2)), dma((7,)),
    ]
    tg, gg, dg, du, dd = pl.pallas_call(
        kernel,
        out_shape=(
            jax.ShapeDtypeStruct((TOK, D), BF16),
            jax.ShapeDtypeStruct((2, TOK), F32),
            jax.ShapeDtypeStruct((2, D, FS), F32),
            jax.ShapeDtypeStruct((2, D, FS), F32),
            jax.ShapeDtypeStruct((2, FS, D), F32),
        ),
        in_specs=[hbm, hbm, vmem, vmem, hbm, hbm, hbm],
        out_specs=(hbm, vmem, hbm, hbm, hbm),
        scratch_shapes=scratch,
        compiler_params=pltpu.CompilerParams(
            collective_id=0, has_side_effects=True, vmem_limit_bytes=63 * 1024 * 1024
        ),
    )(tokens, cotangent, routing.T, gate_weights.T, gate_proj, up_proj, down_proj)
    return tg, gg.T, dg, du, dd


def solution(mesh):
    in_specs = (
        P("ep", None),
        P("ep", None),
        P("ep", None),
        P("ep", None),
        P("ep", None, "tp"),
        P("ep", None, "tp"),
        P("ep", "tp", None),
    )
    out_specs = (
        P("ep", None),
        P("ep", None),
        P("ep", None, "tp"),
        P("ep", None, "tp"),
        P("ep", "tp", None),
    )
    return jax.shard_map(shards, mesh=mesh, in_specs=in_specs, out_specs=out_specs, check_vma=False)
```

profile of v0, /device:TPU:10, one launch (start us, length us, event | category | flops | bytes accessed | tf_op | source)
XLA Modules:
  0.0 129.9 jit_solution(6063151726571449644)
XLA Ops:
  0.6 122.5 %shard_map.110 = (bf16[256,1024]{1,0:T(8,128)(2,1)}, f32[2,256]{1,0:T(2,128)}, f32[2,1024,128]{2,1,0:T(8,128)}, f32[2,1024,128]{2,1,0:T(8,128)}, f32[2,128,1024]{2,1,0:T(8,128)}) custom-call(bf16[256,1024]{1,0:T(8,128)(2,1)} %tok.1, bf16[256,1024]{1,0:T(8,128)(2,1)} %cot.1, s32[2,256]{1,0:T(2,128)} %bitcast.3, f32[2,256]{1,0:T(2,128)} %bitcast.4, ...), custom_call_target="tpu_custom_call" | custom-call | tf_op jit(solution)/shard_map/pallas_call | solution.py:573
  123.2 0.0 copy-start.2
  123.2 0.0 copy-start.3
  123.2 2.0 %copy.17 = bf16[256,1024]{1,0:T(8,128)(2,1)} copy(bf16[256,1024]{1,0:T(8,128)(2,1)} %get-tuple-element.20) | data formatting | bytes 1048576
  125.2 0.0 copy-done.3
  125.2 0.6 copy.18
  125.7 0.0 copy-done.2
  125.7 0.0 copy-start.1
  125.7 1.0 copy.19
  126.7 0.6 copy-done.1
  127.3 0.0 copy-start
  127.3 1.0 copy.20
  128.3 0.6 copy-done
  129.0 1.0 copy.21
Async XLA Ops:
  123.2 2.6 %copy-start.2 = (f32[2,1024,128]{2,1,0:T(8,128)S(1)}, f32[2,1024,128]{2,1,0:T(8,128)}, u32[]{:S(2)}) copy-start(f32[2,1024,128]{2,1,0:T(8,128)} %get-tuple-element.22) | copy-start | bytes 3145732
  123.2 2.0 %copy-start.3 = (f32[2,256]{1,0:T(2,128)S(1)}, f32[2,256]{1,0:T(2,128)}, u32[]{:S(2)}) copy-start(f32[2,256]{1,0:T(2,128)} %get-tuple-element.11) | copy-start | bytes 6148
  125.7 1.6 %copy-start.1 = (f32[2,1024,128]{2,1,0:T(8,128)S(1)}, f32[2,1024,128]{2,1,0:T(8,128)}, u32[]{:S(2)}) copy-start(f32[2,1024,128]{2,1,0:T(8,128)} %get-tuple-element.23) | copy-start | bytes 3145732
  127.3 1.6 %copy-start = (f32[2,128,1024]{2,1,0:T(8,128)S(1)}, f32[2,128,1024]{2,1,0:T(8,128)}, u32[]{:S(2)}) copy-start(f32[2,128,1024]{2,1,0:T(8,128)} %get-tuple-element.24) | copy-start | bytes 3145732
where the time goes:
time: 131 us; the launch traced here: 130 us
  Pallas kernels  123 us (94%)
  local copies, waits for them, and re-layouts  6.71 us (5%)
    pallas_call x1, Pallas kernels, shards(): pl.pallas_call(kernel, out_shape=(jax.ShapeDtypeStruct((TOK, D), BF16), j...  123 us
    unnamed x13, local copies, waits for them, and re-layouts  6.71 us

commit v1 on v0

v1 whole, which is shorter than its diff:
```python
import jax
import jax.numpy as jnp
from jax import lax
from jax.experimental import pallas as pl
from jax.experimental.pallas import tpu as pltpu
from jax.sharding import PartitionSpec as P

F32 = jnp.float32
BF16 = jnp.bfloat16
I32 = jnp.int32
MESH = pl.DeviceIdType.MESH

NZ, NY, NC, NX = 8, 4, 2, 4
PLANE = NY * NC
TOK = 256
D = 1024
Q = 256
FS = 128
CAP = 12
SLOT = 2 * CAP
ROWS = PLANE * SLOT
ALL = NZ * ROWS
POS = {0: 0, 1: 1, 7: 2, 2: 3, 6: 4, 3: 5, 5: 6, 4: 7}
BRINGS = {
    0: (0, 3), 1: (0, 3, 2), 2: (0, 3), 3: (0, 3), 4: (0,), 5: (0, 3), 6: (0, 3), 7: (0, 3, 1),
}
HELD = [(0, k) for k in range(4)]
HELD += [(dz, k) for dz in range(1, NZ) for k in BRINGS[dz]]
HELD = {key: i for i, key in enumerate(HELD)}
BUILT = {key: i for i, key in enumerate((dz, k) for dz in range(NZ) for k in BRINGS[dz])}
PART = TOK // 4
CONTRACT_MINOR = (((1,), (1,)), ((), ()))
CONTRACT_MAJOR = (((0,), (0,)), ((), ()))


def kernel(
    tok, cot, rt, gw, wg, wu, wd,
    tg_out, gg_out, dg_out, du_out, dd_out,
    bk, rb, sx, rq, wv, wgu, wds, wq, sl, upper, pk, wt, ts, gu2, h2,
    gx, pr, prx, prs, prr, pb, pe, igs, igr, db, rm, rp, tq, dg, du, dd,
    in_s, z_s, z_r, rb_s, rb_r, ip_s, ip_r, x_s, x_r, xf_s, xf_r, w_s, w_r, g_s, g_r, gf_s, gf_r,
    p_s, p_r, pp_s, pp_r, pz_s, pz_r, ig_s, ig_r, c_s, c_r, t_s, t_r, out_s,
):
    e = lax.axis_index("ep")
    x = lax.axis_index("tp")
    z = e // PLANE
    y = (e % PLANE) // NC
    c = e % NC

    def at_z(step):
        return (((z + step) % NZ) * PLANE + y * NC + c, x)

    def at_plane(j, sign):
        dy, dc = j // NC, j % NC
        return (z * PLANE + ((y + sign * dy + NY) % NY) * NC + (c + dc) % NC, x)

    def at_x(step):
        return (e, (x + step) % NX)

    def remote(src, dst, ssem, rsem, dev):
        return pltpu.make_async_remote_copy(
            src_ref=src, dst_ref=dst, send_sem=ssem, recv_sem=rsem,
            device_id=dev, device_id_type=MESH,
        )

    def done(ref, sem):
        pltpu.make_async_copy(ref, ref, sem).wait()

    sends = []

    def push(src, dst, ssem, rsem, dev, last=True):
        remote(src, dst, ssem, rsem, dev).start()
        if last:
            sends.append((src, ssem))

    def quarter(k):
        who = (x + (0, NX - 1, 1, 2)[k]) % NX
        return 2 * (who % 2) + who // 2

    with jax.named_scope("prologue"):
        barrier = pltpu.get_barrier_semaphore()
        partners = [at_z(k) for k in range(1, NZ)]
        partners += [at_plane(j, 1) for j in range(1, PLANE)]
        partners += [at_x(s) for s in range(1, NX)]
        for dev in partners:
            pl.semaphore_signal(barrier, inc=1, device_id=dev, device_id_type=MESH)

        loads = []
        for k in (0, 3, 1, 2):
            cols = pl.ds(pl.multiple_of(quarter(k) * Q, Q), Q)
            dst = bk.at[HELD[0, k]]
            loads.append(pltpu.make_async_copy(tok.at[:, cols], dst.at[0], in_s.at[2 * k]))
            loads.append(pltpu.make_async_copy(cot.at[:, cols], dst.at[1], in_s.at[2 * k + 1]))
        for i, w in enumerate((wg, wu)):
            loads.append(pltpu.make_async_copy(w, wv.at[i], in_s.at[8 + i]))
        for q in range(4):
            for i in range(2):
                loads.append(
                    pltpu.make_async_copy(
                        wd.at[i, :, pl.ds(q * Q, Q)], wds.at[q, pl.ds(i * FS, FS)], in_s.at[10 + 2 * q + i]
                    )
                )
        for load in loads:
            load.start()
        rb[0] = jnp.concatenate(
            [rt[...].astype(F32), gw[...], jnp.zeros((4, TOK), F32)], axis=0
        )
        upper[...] = (
            lax.broadcasted_iota(I32, (TOK, TOK), 0) < lax.broadcasted_iota(I32, (TOK, TOK), 1)
        ).astype(F32).astype(BF16)
        pr[...] = jnp.zeros_like(pr)
        for load in loads[:4]:
            load.wait()
    with jax.named_scope("barrier"):
        pl.semaphore_wait(barrier, len(partners))

    def first_of(n, lanes):
        i = lax.broadcasted_iota(I32, (n * PLANE, SLOT, lanes), 1)
        return (i < CAP).reshape(n * ROWS, lanes)

    def lane_of_slot(pos):
        i = lax.broadcasted_iota(I32, (PLANE, SLOT, FS), 1)
        l = lax.broadcasted_iota(I32, (PLANE, SLOT, FS), 2)
        return i + 32 * (pos % 4) == l

    def toward(dz, plus):
        return (dz + 1, at_z(1)) if plus else ((dz + NZ - 1) % NZ, at_z(NZ - 1))

    def z_push(dz, k, plus):
        to, dev = toward(dz, plus)
        src, i = bk.at[HELD[dz, k]], HELD[to, k]
        if to == 4:
            a = 0 if plus else 1
            push(src.at[a], bk.at[i, a], z_s.at[a, HELD[dz, k]], z_r.at[a, i], dev)
        else:
            push(src, bk.at[i], z_s.at[0 if plus else 1, HELD[dz, k]], z_r.at[0, i], dev)

    @jax.named_scope("z_take")
    def z_take(dz, k, onward=True):
        i = HELD[dz, k]
        plus = dz < 4
        first = k == 0
        if first:
            done(rb.at[dz], rb_r.at[dz])
            if dz < 4 or dz > 5:
                if dz != 4:
                    rb_push(dz, plus)
        if dz == 4:
            for a in range(2):
                done(bk.at[i, a], z_r.at[a, i])
            return
        done(bk.at[i], z_r.at[0, i])
        if k in BRINGS[toward(dz, plus)[0]]:
            z_push(dz, k, plus)

    def rb_push(dz, plus):
        if plus:
            to, dev, i = dz + 1, at_z(1), 0
        else:
            to, dev, i = (dz + NZ - 1) % NZ, at_z(NZ - 1), 1
        push(rb.at[dz], rb.at[to], rb_s.at[i, dz], rb_r.at[to], dev)

    @jax.named_scope("slots_of")
    def slots_of(dz):
        pos = POS[dz]
        e16 = lax.broadcasted_iota(I32, (16, TOK), 0)
        target = ((e16 // 4 - y) & 3) * NC + (((e16 // 2) - c) & 1)
        base = (target * SLOT + (e16 & 1) * CAP).astype(F32)
        block = rb[dz]
        chosen = block[0:2].astype(I32) - z * 16
        e0 = (e16 == chosen[0:1]).astype(F32)
        e1 = (e16 == chosen[1:2]).astype(F32)
        both = jnp.concatenate([e0, e1], axis=0).astype(BF16)
        before = jnp.dot(both, upper[...], preferred_element_type=F32)
        before0 = before[0:16]
        before1 = before[16:32] + jnp.sum(e0, axis=1, keepdims=True)
        s0 = jnp.sum(e0 * (base + before0 + 1.0), axis=0, keepdims=True) - 1.0
        s1 = jnp.sum(e1 * (base + before1 + 1.0), axis=0, keepdims=True) - 1.0
        slots = jnp.concatenate([s0, s1], axis=0).astype(I32)
        sl[pos, 0:2] = slots
        row = lax.broadcasted_iota(I32, (ROWS, TOK), 0)
        p0 = row == slots[0:1]
        p1 = row == slots[1:2]
        pk[pos] = (p0 | p1).astype(F32).astype(BF16)
        weight = jnp.sum(
            jnp.where(p0, block[2:3], 0.0) + jnp.where(p1, block[3:4], 0.0),
            axis=1, keepdims=True,
        )
        wt[pos] = jnp.broadcast_to(weight, (ROWS, FS))

    @jax.named_scope("build")
    def build(dz, k):
        pos, b = POS[dz], BUILT[dz, k]
        src, stage, land = bk.at[HELD[dz, k]], sx.at[b], rq.at[k, pos]
        pick = pk[pos]
        w = jnp.concatenate([wt[pos], wt[pos]], axis=1)
        t = jnp.dot(pick, src[0], preferred_element_type=F32)
        s = jnp.dot(pick, src[1], preferred_element_type=F32) * w
        t = t.reshape(PLANE, 3, 8, Q).astype(BF16)
        s = s.reshape(PLANE, 3, 8, Q).astype(BF16)
        stage[:, 0:3] = t
        stage[:, 3:6] = s
        land[0, 0:3] = t[0]
        land[0, 3:6] = s[0]
        for j in range(1, PLANE):
            push(stage.at[j], land.at[j], ip_s.at[b], ip_r.at[b], at_plane(j, 1), last=False)
        sends.append((stage.at[pl.ds(1, PLANE - 1)], ip_s.at[b]))

    def landed(dz, k):
        done(rq.at[k, POS[dz], pl.ds(1, PLANE - 1)], ip_r.at[BUILT[dz, k]])

    @jax.named_scope("x_push")
    def x_push(dz):
        pos = POS[dz]
        landed(dz, 0)
        if 1 not in BRINGS[dz]:
            push(rq.at[0, pos], rq.at[1, pos], x_s.at[0, pos], x_r.at[0, pos], at_x(1))
        if 2 not in BRINGS[dz]:
            push(rq.at[0, pos], rq.at[2, pos], x_s.at[1, pos], x_r.at[1, pos], at_x(NX - 1))

    low, high = pl.ds(0, PLANE // 2), pl.ds(PLANE // 2, PLANE // 2)

    @jax.named_scope("x_pass")
    def x_pass(dz):
        pos = POS[dz]
        done(rq.at[1, pos], x_r.at[0, pos])
        push(rq.at[1, pos, low], rq.at[3, pos, low], xf_s.at[0, pos], xf_r.at[0, pos], at_x(1))
        done(rq.at[2, pos], x_r.at[1, pos])
        push(
            rq.at[2, pos, high], rq.at[3, pos, high], xf_s.at[1, pos], xf_r.at[1, pos],
            at_x(NX - 1),
        )

    @jax.named_scope("compute_wait")
    def compute_wait(*blocks):
        for dz in blocks:
            pos, own = POS[dz], BRINGS[dz]
            for k in own[1:]:
                landed(dz, k)
            if 3 not in own:
                done(rq.at[3, pos, low], xf_r.at[0, pos])
                done(rq.at[3, pos, high], xf_r.at[1, pos])
            else:
                for k in (1, 2):
                    if k not in own:
                        done(rq.at[k, pos], x_r.at[k - 1, pos])

    @jax.named_scope("compute")
    def compute(*blocks):
        p, n = POS[blocks[0]], len(blocks)
        m = n * ROWS
        rows = pl.ds(p * ROWS, m)
        pre = jnp.zeros((m, 512), F32)
        hg = jnp.zeros((m, 256), F32)
        for k in range(4):
            src = rq.at[k]
            t = src[p:p + n, :, 0:3].astype(F32).reshape(m, Q).astype(BF16)
            s = src[p:p + n, :, 3:6].astype(F32).reshape(m, Q).astype(BF16)
            ts[k, 0, rows] = t
            ts[k, 1, rows] = s
            pre = pre + jnp.dot(t, wgu[quarter(k)], preferred_element_type=F32)
            hg = hg + lax.dot_general(
                s, wds[quarter(k)], CONTRACT_MINOR, preferred_element_type=F32
            )
        first = first_of(n, FS)
        g = jnp.where(first, pre[:, 0:128], pre[:, 128:256]).astype(BF16).astype(F32)
        u = jnp.where(first, pre[:, 256:384], pre[:, 384:512]).astype(BF16).astype(F32)
        dh = jnp.where(first, hg[:, 0:128], hg[:, 128:256])
        sg = jax.nn.sigmoid(g)
        act = g * sg
        hidden = act * u
        product = jnp.sum(dh * hidden, axis=1, keepdims=True)
        for i in range(n):
            spread = jnp.broadcast_to(product[i * ROWS:(i + 1) * ROWS], (ROWS, FS))
            placed = jnp.where(lane_of_slot(p + i), spread.reshape(PLANE, SLOT, FS), 0.0)
            pr[(p + i) // 4] += jnp.sum(placed, axis=1)
        gg = dh * u * sg * (1.0 + g * (1.0 - sg))
        ug = dh * act
        gx[0, rows, 0:FS] = gg.astype(BF16)
        gx[0, rows, FS:2 * FS] = ug.astype(BF16)
        for i, v in enumerate((gg, ug, hidden)):
            lo = jnp.where(first, v, 0.0).astype(BF16)
            hi = jnp.where(first, 0.0, v).astype(BF16)
            if i < 2:
                gu2[rows, 256 * i:256 * i + 128] = lo
                gu2[rows, 256 * i + 128:256 * i + 256] = hi
            else:
                h2[rows, 0:128] = lo
                h2[rows, 128:256] = hi

    @jax.named_scope("weight_grads")
    def weight_grads(k):
        at = pl.ds(pl.multiple_of(quarter(k) * Q, Q), Q)
        o = lax.dot_general(ts[k, 0], gu2[...], CONTRACT_MAJOR, preferred_element_type=F32)
        for i in range(2):
            dg[i, at, :] = o[:, i * FS:(i + 1) * FS]
            du[i, at, :] = o[:, 256 + i * FS:256 + (i + 1) * FS]
        o = lax.dot_general(h2[...], ts[k, 1], CONTRACT_MAJOR, preferred_element_type=F32)
        for i in range(2):
            dd[i, :, at] = o[i * FS:(i + 1) * FS]

    def rows_of(dz, lo=0, n=ROWS):
        return pl.ds(POS[dz] * ROWS + lo, n)

    def g_push(dz):
        r = rows_of(dz)
        push(gx.at[0, r], gx.at[1, r], g_s.at[0, dz], g_r.at[0, dz], at_x(1))
        push(gx.at[0, r], gx.at[2, r], g_s.at[1, dz], g_r.at[1, dz], at_x(NX - 1))

    @jax.named_scope("g_pass")
    def g_pass(dz):
        lo, hi = rows_of(dz, 0, 96), rows_of(dz, 96, 96)
        done(gx.at[1, rows_of(dz)], g_r.at[0, dz])
        push(gx.at[1, lo], gx.at[3, lo], gf_s.at[0, dz], gf_r.at[0, dz], at_x(1))
        done(gx.at[2, rows_of(dz)], g_r.at[1, dz])
        push(gx.at[2, hi], gx.at[3, hi], gf_s.at[1, dz], gf_r.at[1, dz], at_x(NX - 1))

    @jax.named_scope("ig_wait")
    def ig_wait(dz):
        done(gx.at[3, rows_of(dz, 0, 96)], gf_r.at[0, dz])
        done(gx.at[3, rows_of(dz, 96, 96)], gf_r.at[1, dz])

    @jax.named_scope("input_grad")
    def input_grad(dz):
        pos = POS[dz]
        first = first_of(1, FS)
        total = jnp.zeros((ROWS, Q), F32)
        for slot, w in ((0, None), (1, 0), (2, 2), (3, 1)):
            pair = gx[slot, rows_of(dz)].astype(F32)
            gg, ug = pair[:, 0:FS], pair[:, FS:2 * FS]
            lhs = jnp.concatenate(
                [
                    jnp.where(first, gg, 0.0).astype(BF16),
                    jnp.where(first, 0.0, gg).astype(BF16),
                    jnp.where(first, ug, 0.0).astype(BF16),
                    jnp.where(first, 0.0, ug).astype(BF16),
                ],
                axis=1,
            )
            rhs = wgu[x] if w is None else wq[w]
            total = total + lax.dot_general(lhs, rhs, CONTRACT_MINOR, preferred_element_type=F32)
        igs[pos] = total
        igr[pos, 0:SLOT] = total[0:SLOT]
        for j in range(1, PLANE):
            at = pl.ds(j * SLOT, SLOT)
            push(
                igs.at[pos, at], igr.at[pos, at], ig_s.at[pos], ig_r.at[pos], at_plane(j, -1),
                last=False,
            )
        sends.append((igs.at[pos, pl.ds(SLOT, ROWS - SLOT)], ig_s.at[pos]))

    @jax.named_scope("dense")
    def dense(dz):
        pos = POS[dz]
        with jax.named_scope("dense_wait"):
            done(igr.at[pos, pl.ds(SLOT, ROWS - SLOT)], ig_r.at[pos])
        pick = pk[pos]
        v = igr[pos]
        hi = v.astype(BF16)
        rest = v - hi.astype(F32)
        mid = rest.astype(BF16)
        low = (rest - mid.astype(F32)).astype(BF16)
        total = lax.dot_general(pick, hi, CONTRACT_MAJOR, preferred_element_type=F32)
        total = total + (
            lax.dot_general(pick, mid, CONTRACT_MAJOR, preferred_element_type=F32)
            + lax.dot_general(pick, low, CONTRACT_MAJOR, preferred_element_type=F32)
        )
        db[dz] = total

    @jax.named_scope("pair_products")
    def pair_products(dz):
        pos = POS[dz]
        row = lax.broadcasted_iota(I32, (ROWS, TOK), 0)
        slots = sl[pos, 0:2]
        spread = jnp.broadcast_to(prr[:, pos // 4][:, None, :], (PLANE, SLOT, FS))
        col = jnp.sum(
            jnp.where(lane_of_slot(pos), spread, 0.0).reshape(ROWS, FS), axis=1, keepdims=True
        )
        r0 = jnp.sum(jnp.where(row == slots[0:1], col, 0.0), axis=0, keepdims=True)
        r1 = jnp.sum(jnp.where(row == slots[1:2], col, 0.0), axis=0, keepdims=True)
        pb[dz] = jnp.concatenate([r0, r1, jnp.zeros((6, Q), F32)], axis=0)
        if dz:
            push(pb.at[dz], pe.at[dz], pz_s.at[dz], pz_r.at[dz], at_z(NZ - dz))

    def part(i):
        return pl.ds(PART * i, PART)

    @jax.named_scope("chain")
    def chain(dz, i):
        if dz < 4 or (dz == 4 and i < 2):
            land, at, dev = rm.at[dz - 1, part(i)], dz - 1, at_z(NZ - 1)
            if dz < 3 or (dz == 3 and i < 2):
                done(rm.at[dz, part(i)], c_r.at[i, dz])
                db[dz, part(i)] += rm[dz, part(i)]
        else:
            land, at, dev = rp.at[dz - 4, part(i)], dz, at_z(1)
            if dz > 5 or (dz == 5 and i >= 2):
                done(rp.at[dz - 5, part(i)], c_r.at[i, dz - 1])
                db[dz, part(i)] += rp[dz - 5, part(i)]
        push(db.at[dz, part(i)], land, c_s.at[i, dz], c_r.at[i, at], dev)

    for plus in (True, False):
        z_push(0, 0, plus)
        rb_push(0, plus)
    slots_of(0)
    for load in loads[4:10]:
        load.wait()
    for k in BRINGS[0]:
        build(0, k)
    with jax.named_scope("weights"):
        for q in range(4):
            for w in range(2):
                for i in range(2):
                    lane = 256 * w + FS * i
                    wgu[q, :, lane:lane + FS] = wv[w, i, q * Q:(q + 1) * Q, :]
        for s in range(1, NX):
            push(wgu.at[(x + s) % NX], wq.at[s - 1], w_s.at[s - 1], w_r.at[s - 1], at_x(s))
        for load in loads[10:]:
            load.wait()

    def take(blocks, k):
        for dz in blocks:
            z_take(dz, k)

    def make(blocks, k):
        for dz in blocks:
            if k == 0:
                slots_of(dz)
            build(dz, k)

    take((1, 7), 0)
    make((1, 7), 0)
    x_push(0)
    take((2, 6), 0)
    z_push(0, 3, True)
    z_push(0, 3, False)
    make((2, 6), 0)
    x_push(1)
    x_push(7)
    compute_wait(0)
    compute(0)
    x_push(2)
    x_push(6)
    take((3, 5), 0)
    make((3, 5), 0)
    take((1, 7), 3)
    make((1, 7), 3)
    x_push(3)
    x_push(5)
    take((4,), 0)
    make((4,), 0)
    x_push(4)
    take((2, 6), 3)
    make((2, 6), 3)
    z_push(0, 2, True)
    z_push(0, 1, False)
    compute_wait(2, 6)
    compute(2, 6)
    x_pass(4)
    g_push(2)
    take((3, 5), 3)
    make((3, 5), 3)
    compute_wait(4)
    compute(4)
    g_push(4)
    g_push(6)
    g_pass(2)
    z_take(1, 2)
    z_take(7, 1)
    build(1, 2)
    build(7, 1)
    compute_wait(3, 5)
    compute(3, 5)
    g_push(3)
    g_pass(4)
    with jax.named_scope("wq_wait"):
        for i in range(NX - 1):
            done(wq.at[i], w_r.at[i])

    def grad(dz):
        ig_wait(dz)
        input_grad(dz)

    g_push(5)
    g_pass(6)
    grad(2)
    grad(4)
    compute_wait(1, 7)
    compute(1, 7)
    g_push(1)

    for s in range(1, NX):
        push(pr, prx.at[s - 1], p_s.at[s - 1], p_r.at[s - 1], at_x(s))

    def products():
        with jax.named_scope("products"):
            for s in range(NX - 1):
                done(prx.at[s], p_r.at[s])
            total = pr[...] + prx[0] + prx[1] + prx[2]
            for j in range(PLANE):
                prs[j] = total[:, j]
            prr[0] = total[:, 0]
            for j in range(1, PLANE):
                push(prs.at[j], prr.at[j], pp_s, pp_r, at_plane(j, -1), last=False)
            sends.append((prs.at[pl.ds(1, PLANE - 1)], pp_s))

    outs = []

    def put(src, dst, sem):
        copy = pltpu.make_async_copy(src, dst, sem)
        copy.start()
        outs.append(copy)

    def early(dz):
        for i in (0, 1):
            chain(dz, 2 + i if dz < 4 else i)

    def later(dz):
        for i in (0, 1):
            chain(dz, i if dz < 4 else 2 + i)

    g_pass(3)
    g_push(7)
    grad(6)
    g_pass(5)
    g_push(0)
    dense(4)
    for i in range(4):
        chain(4, i)
    products()
    grad(3)
    dense(2)
    dense(6)
    g_pass(1)
    weight_grads(0)
    grad(5)
    dense(3)
    early(3)
    later(3)
    g_pass(7)
    with jax.named_scope("products_wait"):
        done(prr.at[pl.ds(1, PLANE - 1)], pp_r)
    for dz in (4, 3, 5):
        pair_products(dz)
    dense(5)
    early(5)
    later(5)
    g_pass(0)
    grad(1)
    weight_grads(1)
    early(2)
    grad(7)
    early(6)
    grad(0)
    later(2)
    dense(1)
    early(1)
    later(6)
    weight_grads(2)
    dense(7)
    early(7)
    weight_grads(3)
    put(dg, dg_out, out_s.at[0])
    put(du, du_out, out_s.at[1])
    put(dd, dd_out, out_s.at[2])
    dense(0)
    later(1)
    later(7)
    for dz in (2, 6, 1, 7, 0):
        pair_products(dz)
    with jax.named_scope("early_final"):
        for i in (0, 1):
            done(rm.at[0, part(2 + i)], c_r.at[2 + i, 0])
            db[0, part(2 + i)] += rm[0, part(2 + i)]
            done(rp.at[3, part(i)], c_r.at[i, 7])
            db[0, part(i)] += rp[3, part(i)]

    mine = pl.ds(pl.multiple_of(x * Q, Q), Q)
    with jax.named_scope("final"):
        for i in (0, 2, 1, 3):
            got, sem = (rm.at[0], c_r.at[i, 0]) if i < 2 else (rp.at[3], c_r.at[i, 7])
            done(got.at[part(i)], sem)
            tq[part(i)] = (db[0, part(i)] + got[part(i)]).astype(BF16)
            src, dst = tq.at[part(i)], tg_out.at[part(i), mine]
            for k in range(1, NX):
                push(src, dst, t_s.at[k - 1, i], t_r.at[k - 1, i], at_x(k))
        put(tq, tg_out.at[:, mine], out_s.at[3])
        total = pb[0]
        for dz in range(1, NZ):
            done(pe.at[dz], pz_r.at[dz])
            total = total + pe[dz]
        gg_out[...] = total[0:2] / gw[...]
    with jax.named_scope("gather"):
        for k in range(1, NX):
            theirs = pl.ds(pl.multiple_of((x + NX - k) % NX * Q, Q), Q)
            for i in range(4):
                done(tg_out.at[part(i), theirs], t_r.at[k - 1, i])
    with jax.named_scope("drain"):
        for src, sem in sends:
            done(src, sem)
        for copy in outs:
            copy.wait()


def carry(tg, gg, dg, du, dd, tg_out, gg_out, dg_out, du_out, dd_out, tg_v, w_v, d_v, in_s, out_s):
    pairs = [(tg, tg_v, tg_out)]
    for i, (a, b) in enumerate(((dg, dg_out), (du, du_out), (dd, dd_out))):
        for k in range(2):
            pairs.append((a.at[k], w_v.at[2 * i + k] if i < 2 else d_v.at[k], b.at[k]))
    views = []
    for i, (a, v, b) in enumerate(pairs):
        views.append((pltpu.make_async_copy(a, v, in_s.at[i]), pltpu.make_async_copy(v, b, out_s.at[i])))
    for load, _ in views:
        load.start()
    gg_out[...] = gg[...]
    for load, store in views:
        load.wait()
        store.start()
    for _, store in views:
        store.wait()


def shards(tokens, cotangent, routing, gate_weights, gate_proj, up_proj, down_proj):
    vmem = pl.BlockSpec(memory_space=pltpu.VMEM)
    hbm = pl.BlockSpec(memory_space=pl.ANY)
    dma = pltpu.SemaphoreType.DMA
    scratch = [
        pltpu.VMEM((len(HELD), 2, TOK, Q), BF16),
        pltpu.VMEM((NZ, 8, TOK), F32),
        pltpu.VMEM((len(BUILT), PLANE, 6, 8, Q), BF16),
        pltpu.VMEM((4, NZ, PLANE, 6, 8, Q), BF16),
        pltpu.VMEM((2, 2, D, FS), BF16),
        pltpu.VMEM((4, Q, 512), BF16),
        pltpu.VMEM((4, 256, Q), BF16),
        pltpu.VMEM((3, Q, 512), BF16),
        pltpu.VMEM((NZ, 8, TOK), I32),
        pltpu.VMEM((TOK, TOK), BF16),
        pltpu.VMEM((NZ, ROWS, TOK), BF16),
        pltpu.VMEM((NZ, ROWS, FS), F32),
        pltpu.VMEM((4, 2, ALL, Q), BF16),
        pltpu.VMEM((ALL, 512), BF16),
        pltpu.VMEM((ALL, 256), BF16),
        pltpu.VMEM((4, ALL, 256), BF16),
        pltpu.VMEM((2, PLANE, FS), F32),
        pltpu.VMEM((3, 2, PLANE, FS), F32),
        pltpu.VMEM((PLANE, 2, FS), F32),
        pltpu.VMEM((PLANE, 2, FS), F32),
        pltpu.VMEM((NZ, 8, Q), F32),
        pltpu.VMEM((NZ, 8, Q), F32),
        pltpu.VMEM((NZ, ROWS, Q), F32),
        pltpu.VMEM((NZ, ROWS, Q), F32),
        pltpu.VMEM((NZ, TOK, Q), F32),
        pltpu.VMEM((4, TOK, Q), F32),
        pltpu.VMEM((4, TOK, Q), F32),
        pltpu.VMEM((TOK, Q), BF16),
        pltpu.VMEM((2, D, FS), F32),
        pltpu.VMEM((2, D, FS), F32),
        pltpu.VMEM((2, FS, D), F32),
        dma((18,)), dma((2, len(HELD))), dma((2, len(HELD))), dma((2, 8)), dma((8,)),
        dma((len(BUILT),)), dma((len(BUILT),)),
        dma((2, 8)), dma((2, 8)), dma((2, 8)), dma((2, 8)),
        dma((3,)), dma((3,)), dma((2, 8)), dma((2, 8)), dma((2, 8)), dma((2, 8)),
        dma((3,)), dma((3,)), dma, dma, dma((8,)), dma((8,)), dma((8,)), dma((8,)),
        dma((4, 8)), dma((4, 8)), dma((3, 4)), dma((3, 4)), dma((7,)),
    ]
    tg, gg, dg, du, dd = pl.pallas_call(
        kernel,
        out_shape=(
            jax.ShapeDtypeStruct((TOK, D), BF16),
            jax.ShapeDtypeStruct((2, TOK), F32),
            jax.ShapeDtypeStruct((2, D, FS), F32),
            jax.ShapeDtypeStruct((2, D, FS), F32),
            jax.ShapeDtypeStruct((2, FS, D), F32),
        ),
        in_specs=[hbm, hbm, vmem, vmem, hbm, hbm, hbm],
        out_specs=(hbm, vmem, hbm, hbm, hbm),
        scratch_shapes=scratch,
        compiler_params=pltpu.CompilerParams(
            collective_id=0, has_side_effects=True, vmem_limit_bytes=63 * 1024 * 1024
        ),
    )(tokens, cotangent, routing.T, gate_weights.T, gate_proj, up_proj, down_proj)
    wide = jax.ShapeDtypeStruct((2, D, FS), F32)
    tg, gg, dg, du, dd = pl.pallas_call(
        carry,
        out_shape=(
            jax.ShapeDtypeStruct((TOK, D), BF16),
            jax.ShapeDtypeStruct((2, TOK), F32),
            wide, wide,
            jax.ShapeDtypeStruct((2, FS, D), F32),
        ),
        in_specs=[hbm, vmem, hbm, hbm, hbm],
        out_specs=(hbm, vmem, hbm, hbm, hbm),
        scratch_shapes=[
            pltpu.VMEM((TOK, D), BF16),
            pltpu.VMEM((4, D, FS), F32),
            pltpu.VMEM((2, FS, D), F32),
            dma((7,)),
            dma((7,)),
        ],
        compiler_params=pltpu.CompilerParams(vmem_limit_bytes=63 * 1024 * 1024),
    )(tg, gg, dg, du, dd)
    return tg, gg.T, dg, du, dd


def solution(mesh):
    in_specs = (
        P("ep", None),
        P("ep", None),
        P("ep", None),
        P("ep", None),
        P("ep", None, "tp"),
        P("ep", None, "tp"),
        P("ep", "tp", None),
    )
    out_specs = (
        P("ep", None),
        P("ep", None),
        P("ep", None, "tp"),
        P("ep", None, "tp"),
        P("ep", "tp", None),
    )
    return jax.shard_map(shards, mesh=mesh, in_specs=in_specs, out_specs=out_specs, check_vma=False)
```

time: 131 us -> 122 us (0.931)
  local copies, waits for them, and re-layouts: 6.71 us -> 0 us
  Pallas kernels: 123 us -> 121 us
    unnamed x13 -> x0, local copies, waits for them, and re-layouts: 6.71 us -> none
    pallas_call x1, Pallas kernels: 123 us -> 117 us  [shards(): pl.pallas_call(kernel, out_shape=(jax.ShapeDtypeStruct((TOK, D), BF16), j...]
    pallas_call x0 -> x1, Pallas kernels: none -> 4.27 us  [shards(): pl.pallas_call(carry, out_shape=(jax.ShapeDtypeStruct((TOK, D), BF16), ja...]
where the time goes in v1:
time: 122 us
  Pallas kernels  121 us (99%)
    pallas_call x1, Pallas kernels, shards(): pl.pallas_call(kernel, out_shape=(jax.ShapeDtypeStruct((TOK, D), BF16), j...  117 us
    pallas_call x1, Pallas kernels, shards(): pl.pallas_call(carry, out_shape=(jax.ShapeDtypeStruct((TOK, D), BF16), ja...  4.27 us

profile of v1, /device:TPU:10, one launch (start us, length us, event | category | flops | bytes accessed | tf_op | source)
XLA Modules:
  0.0 121.6 jit_solution(10402346138163388382)
XLA Ops:
  0.6 116.6 %shard_map.110 = (bf16[256,1024]{1,0:T(8,128)(2,1)}, f32[2,256]{1,0:T(2,128)}, f32[2,1024,128]{2,1,0:T(8,128)}, f32[2,1024,128]{2,1,0:T(8,128)}, f32[2,128,1024]{2,1,0:T(8,128)}) custom-call(bf16[256,1024]{1,0:T(8,128)(2,1)} %tok.1, bf16[256,1024]{1,0:T(8,128)(2,1)} %cot.1, s32[2,256]{1,0:T(2,128)} %bitcast.3, f32[2,256]{1,0:T(2,128)} %bitcast.4, ...), custom_call_target="tpu_custom_call" | custom-call | tf_op jit(solution)/shard_map/pallas_call | solution.py:666
  117.2 4.3 %shard_map.111 = (bf16[256,1024]{1,0:T(8,128)(2,1)}, f32[2,256]{1,0:T(2,128)}, f32[2,1024,128]{2,1,0:T(8,128)}, f32[2,1024,128]{2,1,0:T(8,128)}, f32[2,128,1024]{2,1,0:T(8,128)}) custom-call(bf16[256,1024]{1,0:T(8,128)(2,1)} %get-tuple-element.15.tg, f32[2,256]{1,0:T(2,128)} %get-tuple-element.16.gg, f32[2,1024,128]{2,1,0:T(8,128)} %get-tuple-element.17.dg, ...), custom_call_target="tpu_custom_call" | custom-call | tf_op jit(solution)/shard_map/pallas_call | solution.py:683

commit v2 on v1

--- a/solution.py
+++ b/solution.py
@@ -25,7 +25,7 @@
     0: (0, 3), 1: (0, 3, 2), 2: (0, 3), 3: (0, 3), 4: (0,), 5: (0, 3), 6: (0, 3), 7: (0, 3, 1),
 }
 HELD = [(0, k) for k in range(4)]
-HELD += [(dz, k) for dz in range(1, NZ) for k in BRINGS[dz]]
+HELD += [(dz, k) for dz in (1, 2, 3, 5, 6, 7, 4) for k in BRINGS[dz]]
 HELD = {key: i for i, key in enumerate(HELD)}
 BUILT = {key: i for i, key in enumerate((dz, k) for dz in range(NZ) for k in BRINGS[dz])}
 PART = TOK // 4
@@ -34,9 +34,9 @@
 
 
 def kernel(
-    tok, cot, rt, gw, wg, wu, wd,
+    tok, cot, rt_in, gw_in, wg, wu, wd,
     tg_out, gg_out, dg_out, du_out, dd_out,
-    bk, rb, sx, rq, wv, wgu, wds, wq, sl, upper, pk, wt, ts, gu2, h2,
+    rt, gw, gg, bk, rb, sx, rq, wv, wgu, wds, wq, sl, upper, pk, wt, ts, gu2, h2,
     gx, pr, prx, prs, prr, pb, pe, igs, igr, db, rm, rp, tq, dg, du, dd,
     in_s, z_s, z_r, rb_s, rb_r, ip_s, ip_r, x_s, x_r, xf_s, xf_r, w_s, w_r, g_s, g_r, gf_s, gf_r,
     p_s, p_r, pp_s, pp_r, pz_s, pz_r, ig_s, ig_r, c_s, c_r, t_s, t_r, out_s,
@@ -66,12 +66,8 @@
     def done(ref, sem):
         pltpu.make_async_copy(ref, ref, sem).wait()
 
-    sends = []
-
-    def push(src, dst, ssem, rsem, dev, last=True):
+    def push(src, dst, ssem, rsem, dev):
         remote(src, dst, ssem, rsem, dev).start()
-        if last:
-            sends.append((src, ssem))
 
     def quarter(k):
         who = (x + (0, NX - 1, 1, 2)[k]) % NX
@@ -85,32 +81,36 @@
         for dev in partners:
             pl.semaphore_signal(barrier, inc=1, device_id=dev, device_id_type=MESH)
 
-        loads = []
+        loads = [
+            pltpu.make_async_copy(rt_in, rt, in_s.at[0]),
+            pltpu.make_async_copy(gw_in, gw, in_s.at[1]),
+        ]
         for k in (0, 3, 1, 2):
             cols = pl.ds(pl.multiple_of(quarter(k) * Q, Q), Q)
             dst = bk.at[HELD[0, k]]
-            loads.append(pltpu.make_async_copy(tok.at[:, cols], dst.at[0], in_s.at[2 * k]))
-            loads.append(pltpu.make_async_copy(cot.at[:, cols], dst.at[1], in_s.at[2 * k + 1]))
+            loads.append(pltpu.make_async_copy(tok.at[:, cols], dst.at[0], in_s.at[2 if k in (0, 3) else 3]))
+            loads.append(pltpu.make_async_copy(cot.at[:, cols], dst.at[1], in_s.at[2 if k in (0, 3) else 3]))
         for i, w in enumerate((wg, wu)):
-            loads.append(pltpu.make_async_copy(w, wv.at[i], in_s.at[8 + i]))
+            loads.append(pltpu.make_async_copy(w, wv.at[i], in_s.at[4]))
         for q in range(4):
             for i in range(2):
                 loads.append(
                     pltpu.make_async_copy(
-                        wd.at[i, :, pl.ds(q * Q, Q)], wds.at[q, pl.ds(i * FS, FS)], in_s.at[10 + 2 * q + i]
+                        wd.at[i, :, pl.ds(q * Q, Q)], wds.at[q, pl.ds(i * FS, FS)], in_s.at[5]
                     )
                 )
         for load in loads:
             load.start()
-        rb[0] = jnp.concatenate(
-            [rt[...].astype(F32), gw[...], jnp.zeros((4, TOK), F32)], axis=0
-        )
         upper[...] = (
             lax.broadcasted_iota(I32, (TOK, TOK), 0) < lax.broadcasted_iota(I32, (TOK, TOK), 1)
         ).astype(F32).astype(BF16)
         pr[...] = jnp.zeros_like(pr)
-        for load in loads[:4]:
-            load.wait()
+        loads[0].wait()
+        loads[1].wait()
+        done(bk.at[pl.ds(0, 2)], in_s.at[2])
+        rb[0] = jnp.concatenate(
+            [rt[...].astype(F32), gw[...], jnp.zeros((4, TOK), F32)], axis=0
+        )
     with jax.named_scope("barrier"):
         pl.semaphore_wait(barrier, len(partners))
 
@@ -131,9 +131,9 @@
         src, i = bk.at[HELD[dz, k]], HELD[to, k]
         if to == 4:
             a = 0 if plus else 1
-            push(src.at[a], bk.at[i, a], z_s.at[a, HELD[dz, k]], z_r.at[a, i], dev)
+            push(src.at[a], bk.at[i, a], z_s, z_r.at[i + a], dev)
         else:
-            push(src, bk.at[i], z_s.at[0 if plus else 1, HELD[dz, k]], z_r.at[0, i], dev)
+            push(src, bk.at[i], z_s, z_r.at[i], dev)
 
     @jax.named_scope("z_take")
     def z_take(dz, k, onward=True):
@@ -147,9 +147,9 @@
                     rb_push(dz, plus)
         if dz == 4:
             for a in range(2):
-                done(bk.at[i, a], z_r.at[a, i])
+                done(bk.at[i, a], z_r.at[i + a])
             return
-        done(bk.at[i], z_r.at[0, i])
+        done(bk.at[i], z_r.at[i])
         if k in BRINGS[toward(dz, plus)[0]]:
             z_push(dz, k, plus)
 
@@ -158,7 +158,7 @@
             to, dev, i = dz + 1, at_z(1), 0
         else:
             to, dev, i = (dz + NZ - 1) % NZ, at_z(NZ - 1), 1
-        push(rb.at[dz], rb.at[to], rb_s.at[i, dz], rb_r.at[to], dev)
+        push(rb.at[dz], rb.at[to], rb_s, rb_r.at[to], dev)
 
     @jax.named_scope("slots_of")
     def slots_of(dz):
@@ -203,8 +203,7 @@
         land[0, 0:3] = t[0]
         land[0, 3:6] = s[0]
         for j in range(1, PLANE):
-            push(stage.at[j], land.at[j], ip_s.at[b], ip_r.at[b], at_plane(j, 1), last=False)
-        sends.append((stage.at[pl.ds(1, PLANE - 1)], ip_s.at[b]))
+            push(stage.at[j], land.at[j], ip_s, ip_r.at[b], at_plane(j, 1))
 
     def landed(dz, k):
         done(rq.at[k, POS[dz], pl.ds(1, PLANE - 1)], ip_r.at[BUILT[dz, k]])
@@ -214,9 +213,9 @@
         pos = POS[dz]
         landed(dz, 0)
         if 1 not in BRINGS[dz]:
-            push(rq.at[0, pos], rq.at[1, pos], x_s.at[0, pos], x_r.at[0, pos], at_x(1))
+            push(rq.at[0, pos], rq.at[1, pos], x_s, x_r.at[0, pos], at_x(1))
         if 2 not in BRINGS[dz]:
-            push(rq.at[0, pos], rq.at[2, pos], x_s.at[1, pos], x_r.at[1, pos], at_x(NX - 1))
+            push(rq.at[0, pos], rq.at[2, pos], x_s, x_r.at[1, pos], at_x(NX - 1))
 
     low, high = pl.ds(0, PLANE // 2), pl.ds(PLANE // 2, PLANE // 2)
 
@@ -224,10 +223,10 @@
     def x_pass(dz):
         pos = POS[dz]
         done(rq.at[1, pos], x_r.at[0, pos])
-        push(rq.at[1, pos, low], rq.at[3, pos, low], xf_s.at[0, pos], xf_r.at[0, pos], at_x(1))
+        push(rq.at[1, pos, low], rq.at[3, pos, low], xf_s, xf_r.at[0], at_x(1))
         done(rq.at[2, pos], x_r.at[1, pos])
         push(
-            rq.at[2, pos, high], rq.at[3, pos, high], xf_s.at[1, pos], xf_r.at[1, pos],
+            rq.at[2, pos, high], rq.at[3, pos, high], xf_s, xf_r.at[1],
             at_x(NX - 1),
         )
 
@@ -238,8 +237,8 @@
             for k in own[1:]:
                 landed(dz, k)
             if 3 not in own:
-                done(rq.at[3, pos, low], xf_r.at[0, pos])
-                done(rq.at[3, pos, high], xf_r.at[1, pos])
+                done(rq.at[3, pos, low], xf_r.at[0])
+                done(rq.at[3, pos, high], xf_r.at[1])
             else:
                 for k in (1, 2):
                     if k not in own:
@@ -304,16 +303,16 @@
 
     def g_push(dz):
         r = rows_of(dz)
-        push(gx.at[0, r], gx.at[1, r], g_s.at[0, dz], g_r.at[0, dz], at_x(1))
-        push(gx.at[0, r], gx.at[2, r], g_s.at[1, dz], g_r.at[1, dz], at_x(NX - 1))
+        push(gx.at[0, r], gx.at[1, r], g_s, g_r.at[0, dz], at_x(1))
+        push(gx.at[0, r], gx.at[2, r], g_s, g_r.at[1, dz], at_x(NX - 1))
 
     @jax.named_scope("g_pass")
     def g_pass(dz):
         lo, hi = rows_of(dz, 0, 96), rows_of(dz, 96, 96)
         done(gx.at[1, rows_of(dz)], g_r.at[0, dz])
-        push(gx.at[1, lo], gx.at[3, lo], gf_s.at[0, dz], gf_r.at[0, dz], at_x(1))
+        push(gx.at[1, lo], gx.at[3, lo], gf_s, gf_r.at[0, dz], at_x(1))
         done(gx.at[2, rows_of(dz)], g_r.at[1, dz])
-        push(gx.at[2, hi], gx.at[3, hi], gf_s.at[1, dz], gf_r.at[1, dz], at_x(NX - 1))
+        push(gx.at[2, hi], gx.at[3, hi], gf_s, gf_r.at[1, dz], at_x(NX - 1))
 
     @jax.named_scope("ig_wait")
     def ig_wait(dz):
@@ -344,10 +343,8 @@
         for j in range(1, PLANE):
             at = pl.ds(j * SLOT, SLOT)
             push(
-                igs.at[pos, at], igr.at[pos, at], ig_s.at[pos], ig_r.at[pos], at_plane(j, -1),
-                last=False,
+                igs.at[pos, at], igr.at[pos, at], ig_s, ig_r.at[pos], at_plane(j, -1),
             )
-        sends.append((igs.at[pos, pl.ds(SLOT, ROWS - SLOT)], ig_s.at[pos]))
 
     @jax.named_scope("dense")
     def dense(dz):
@@ -380,7 +377,7 @@
         r1 = jnp.sum(jnp.where(row == slots[1:2], col, 0.0), axis=0, keepdims=True)
         pb[dz] = jnp.concatenate([r0, r1, jnp.zeros((6, Q), F32)], axis=0)
         if dz:
-            push(pb.at[dz], pe.at[dz], pz_s.at[dz], pz_r.at[dz], at_z(NZ - dz))
+            push(pb.at[dz], pe.at[dz], pz_s, pz_r, at_z(NZ - dz))
 
     def part(i):
         return pl.ds(PART * i, PART)
@@ -397,14 +394,39 @@
             if dz > 5 or (dz == 5 and i >= 2):
                 done(rp.at[dz - 5, part(i)], c_r.at[i, dz - 1])
                 db[dz, part(i)] += rp[dz - 5, part(i)]
-        push(db.at[dz, part(i)], land, c_s.at[i, dz], c_r.at[i, at], dev)
+        push(db.at[dz, part(i)], land, c_s, c_r.at[i, at], dev)
+
+    def products():
+        with jax.named_scope("products"):
+            done(prx, p_r)
+            total = pr[...] + prx[0] + prx[1] + prx[2]
+            for j in range(PLANE):
+                prs[j] = total[:, j]
+            prr[0] = total[:, 0]
+            for j in range(1, PLANE):
+                push(prs.at[j], prr.at[j], pp_s, pp_r, at_plane(j, -1))
+
+    def put(src, dst, sem):
+        pltpu.make_async_copy(src, dst, sem).start()
+
+    def early(dz):
+        for i in (0, 1):
+            chain(dz, 2 + i if dz < 4 else i)
+
+    def later(dz):
+        for i in (0, 1):
+            chain(dz, i if dz < 4 else 2 + i)
+
+    def grad(dz):
+        ig_wait(dz)
+        input_grad(dz)
 
     for plus in (True, False):
         z_push(0, 0, plus)
         rb_push(0, plus)
     slots_of(0)
-    for load in loads[4:10]:
-        load.wait()
+    done(bk.at[pl.ds(0, 2)], in_s.at[3])
+    done(wv, in_s.at[4])
     for k in BRINGS[0]:
         build(0, k)
     with jax.named_scope("weights"):
@@ -414,9 +436,8 @@
                     lane = 256 * w + FS * i
                     wgu[q, :, lane:lane + FS] = wv[w, i, q * Q:(q + 1) * Q, :]
         for s in range(1, NX):
-            push(wgu.at[(x + s) % NX], wq.at[s - 1], w_s.at[s - 1], w_r.at[s - 1], at_x(s))
-        for load in loads[10:]:
-            load.wait()
+            push(wgu.at[(x + s) % NX], wq.at[s - 1], w_s, w_r, at_x(s))
+        done(wds, in_s.at[5])
 
     def take(blocks, k):
         for dz in blocks:
@@ -458,116 +479,73 @@
     compute(2, 6)
     x_pass(4)
     g_push(2)
+    g_push(6)
     take((3, 5), 3)
     make((3, 5), 3)
-    compute_wait(4)
-    compute(4)
-    g_push(4)
-    g_push(6)
-    g_pass(2)
     z_take(1, 2)
     z_take(7, 1)
     build(1, 2)
     build(7, 1)
+    g_pass(2)
+    compute_wait(4)
+    compute(4)
+    g_push(4)
     compute_wait(3, 5)
     compute(3, 5)
+    g_pass(6)
     g_push(3)
+    with jax.named_scope("wq_wait"):
+        done(wq, w_r)
+    grad(2)
     g_pass(4)
-    with jax.named_scope("wq_wait"):
-        for i in range(NX - 1):
-            done(wq.at[i], w_r.at[i])
-
-    def grad(dz):
-        ig_wait(dz)
-        input_grad(dz)
-
     g_push(5)
-    g_pass(6)
-    grad(2)
-    grad(4)
+    grad(6)
     compute_wait(1, 7)
     compute(1, 7)
+
+    for s in range(1, NX):
+        push(pr, prx.at[s - 1], p_s, p_r, at_x(s))
+    g_pass(3)
     g_push(1)
-
-    for s in range(1, NX):
-        push(pr, prx.at[s - 1], p_s.at[s - 1], p_r.at[s - 1], at_x(s))
-
-    def products():
-        with jax.named_scope("products"):
-            for s in range(NX - 1):
-                done(prx.at[s], p_r.at[s])
-            total = pr[...] + prx[0] + prx[1] + prx[2]
-            for j in range(PLANE):
-                prs[j] = total[:, j]
-            prr[0] = total[:, 0]
-            for j in range(1, PLANE):
-                push(prs.at[j], prr.at[j], pp_s, pp_r, at_plane(j, -1), last=False)
-            sends.append((prs.at[pl.ds(1, PLANE - 1)], pp_s))
-
-    outs = []
-
-    def put(src, dst, sem):
-        copy = pltpu.make_async_copy(src, dst, sem)
-        copy.start()
-        outs.append(copy)
-
-    def early(dz):
-        for i in (0, 1):
-            chain(dz, 2 + i if dz < 4 else i)
-
-    def later(dz):
-        for i in (0, 1):
-            chain(dz, i if dz < 4 else 2 + i)
-
-    g_pass(3)
+    grad(4)
+    g_pass(5)
     g_push(7)
-    grad(6)
-    g_pass(5)
+    dense(2)
+    dense(6)
+    grad(3)
+    products()
+    g_pass(1)
     g_push(0)
     dense(4)
     for i in range(4):
         chain(4, i)
-    products()
-    grad(3)
-    dense(2)
-    dense(6)
-    g_pass(1)
-    weight_grads(0)
     grad(5)
     dense(3)
     early(3)
+    g_pass(7)
     later(3)
-    g_pass(7)
-    with jax.named_scope("products_wait"):
-        done(prr.at[pl.ds(1, PLANE - 1)], pp_r)
-    for dz in (4, 3, 5):
-        pair_products(dz)
+    grad(1)
     dense(5)
     early(5)
     later(5)
     g_pass(0)
-    grad(1)
-    weight_grads(1)
     early(2)
     grad(7)
+    later(2)
     early(6)
-    grad(0)
-    later(2)
     dense(1)
     early(1)
     later(6)
-    weight_grads(2)
+    grad(0)
+    later(1)
     dense(7)
     early(7)
-    weight_grads(3)
-    put(dg, dg_out, out_s.at[0])
-    put(du, du_out, out_s.at[1])
-    put(dd, dd_out, out_s.at[2])
+    later(7)
+    with jax.named_scope("products_wait"):
+        done(prr.at[pl.ds(1, PLANE - 1)], pp_r)
+    for dz in (4, 3, 5, 2, 6, 1, 7, 0):
+        pair_products(dz)
     dense(0)
-    later(1)
-    later(7)
-    for dz in (2, 6, 1, 7, 0):
-        pair_products(dz)
     with jax.named_scope("early_final"):
         for i in (0, 1):
             done(rm.at[0, part(2 + i)], c_r.at[2 + i, 0])
@@ -583,27 +561,46 @@
             tq[part(i)] = (db[0, part(i)] + got[part(i)]).astype(BF16)
             src, dst = tq.at[part(i)], tg_out.at[part(i), mine]
             for k in range(1, NX):
-                push(src, dst, t_s.at[k - 1, i], t_r.at[k - 1, i], at_x(k))
-        put(tq, tg_out.at[:, mine], out_s.at[3])
-        total = pb[0]
-        for dz in range(1, NZ):
-            done(pe.at[dz], pz_r.at[dz])
-            total = total + pe[dz]
-        gg_out[...] = total[0:2] / gw[...]
+                push(src, dst, t_s, t_r, at_x(k))
+        put(tq, tg_out.at[:, mine], out_s.at[0])
+    for k in range(4):
+        weight_grads(k)
+        at = pl.ds(pl.multiple_of(quarter(k) * Q, Q), Q)
+        put(dg.at[:, at], dg_out.at[:, at], out_s.at[1])
+        put(du.at[:, at], du_out.at[:, at], out_s.at[2])
+        put(dd.at[:, :, at], dd_out.at[:, :, at], out_s.at[3])
+    done(pe.at[pl.ds(1, NZ - 1)], pz_r)
+    total = pb[0]
+    for dz in range(1, NZ):
+        total = total + pe[dz]
+    gg[...] = total[0:2] / gw[...]
+    put(gg, gg_out, out_s.at[4])
     with jax.named_scope("gather"):
-        for k in range(1, NX):
-            theirs = pl.ds(pl.multiple_of((x + NX - k) % NX * Q, Q), Q)
-            for i in range(4):
-                done(tg_out.at[part(i), theirs], t_r.at[k - 1, i])
+        done(gx.at[0, pl.ds(0, 3 * TOK)], t_r)
     with jax.named_scope("drain"):
-        for src, sem in sends:
-            done(src, sem)
-        for copy in outs:
-            copy.wait()
-
-
-def carry(tg, gg, dg, du, dd, tg_out, gg_out, dg_out, du_out, dd_out, tg_v, w_v, d_v, in_s, out_s):
-    pairs = [(tg, tg_v, tg_out)]
+        done(bk.at[pl.ds(0, 15)], z_s)
+        done(rb.at[pl.ds(0, 7)], rb_s)
+        done(sx.at[:, pl.ds(1, PLANE - 1)], ip_s)
+        done(rq.at[pl.ds(0, 2), pl.ds(0, 7)], x_s)
+        done(rq.at[0, 0], xf_s)
+        done(wq, w_s)
+        done(gx.at[pl.ds(0, 2)], g_s)
+        done(gx.at[0], gf_s)
+        done(prx, p_s)
+        done(prs.at[pl.ds(1, PLANE - 1)], pp_s)
+        done(pb.at[pl.ds(0, NZ - 1)], pz_s)
+        done(igs.at[:, pl.ds(SLOT, ROWS - SLOT)], ig_s)
+        done(db.at[pl.ds(0, 7)], c_s)
+        done(gx.at[0, pl.ds(0, 3 * TOK)], t_s)
+        done(tq, out_s.at[0])
+        done(dg, out_s.at[1])
+        done(du, out_s.at[2])
+        done(dd, out_s.at[3])
+        done(gg, out_s.at[4])
+
+
+def carry(tg, gg, dg, du, dd, tg_out, gg_out, dg_out, du_out, dd_out, tg_v, gg_v, w_v, d_v, in_s, out_s):
+    pairs = [(tg, tg_v, tg_out), (gg, gg_v, gg_out)]
     for i, (a, b) in enumerate(((dg, dg_out), (du, du_out), (dd, dd_out))):
         for k in range(2):
             pairs.append((a.at[k], w_v.at[2 * i + k] if i < 2 else d_v.at[k], b.at[k]))
@@ -612,7 +609,6 @@
         views.append((pltpu.make_async_copy(a, v, in_s.at[i]), pltpu.make_async_copy(v, b, out_s.at[i])))
     for load, _ in views:
         load.start()
-    gg_out[...] = gg[...]
     for load, store in views:
         load.wait()
         store.start()
@@ -621,10 +617,12 @@
 
 
 def shards(tokens, cotangent, routing, gate_weights, gate_proj, up_proj, down_proj):
-    vmem = pl.BlockSpec(memory_space=pltpu.VMEM)
     hbm = pl.BlockSpec(memory_space=pl.ANY)
     dma = pltpu.SemaphoreType.DMA
     scratch = [
+        pltpu.VMEM((2, TOK), I32),
+        pltpu.VMEM((2, TOK), F32),
+        pltpu.VMEM((2, TOK), F32),
         pltpu.VMEM((len(HELD), 2, TOK, Q), BF16),
         pltpu.VMEM((NZ, 8, TOK), F32),
         pltpu.VMEM((len(BUILT), PLANE, 6, 8, Q), BF16),
@@ -656,12 +654,12 @@
         pltpu.VMEM((2, D, FS), F32),
         pltpu.VMEM((2, D, FS), F32),
         pltpu.VMEM((2, FS, D), F32),
-        dma((18,)), dma((2, len(HELD))), dma((2, len(HELD))), dma((2, 8)), dma((8,)),
-        dma((len(BUILT),)), dma((len(BUILT),)),
-        dma((2, 8)), dma((2, 8)), dma((2, 8)), dma((2, 8)),
-        dma((3,)), dma((3,)), dma((2, 8)), dma((2, 8)), dma((2, 8)), dma((2, 8)),
-        dma((3,)), dma((3,)), dma, dma, dma((8,)), dma((8,)), dma((8,)), dma((8,)),
-        dma((4, 8)), dma((4, 8)), dma((3, 4)), dma((3, 4)), dma((7,)),
+        dma((6,)), dma, dma((len(HELD) + 1,)), dma, dma((8,)),
+        dma, dma((len(BUILT),)),
+        dma, dma((2, 8)), dma, dma((2,)),
+        dma, dma, dma, dma((2, 8)), dma, dma((2, 8)),
+        dma, dma, dma, dma, dma, dma, dma, dma((8,)),
+        dma, dma((4, 8)), dma, dma, dma((5,)),
     ]
     tg, gg, dg, du, dd = pl.pallas_call(
         kernel,
@@ -672,8 +670,8 @@
             jax.ShapeDtypeStruct((2, D, FS), F32),
             jax.ShapeDtypeStruct((2, FS, D), F32),
         ),
-        in_specs=[hbm, hbm, vmem, vmem, hbm, hbm, hbm],
-        out_specs=(hbm, vmem, hbm, hbm, hbm),
+        in_specs=[hbm] * 7,
+        out_specs=(hbm,) * 5,
         scratch_shapes=scratch,
         compiler_params=pltpu.CompilerParams(
             collective_id=0, has_side_effects=True, vmem_limit_bytes=63 * 1024 * 1024
@@ -688,14 +686,15 @@
             wide, wide,
             jax.ShapeDtypeStruct((2, FS, D), F32),
         ),
-        in_specs=[hbm, vmem, hbm, hbm, hbm],
-        out_specs=(hbm, vmem, hbm, hbm, hbm),
+        in_specs=[hbm] * 5,
+        out_specs=(hbm,) * 5,
         scratch_shapes=[
             pltpu.VMEM((TOK, D), BF16),
+            pltpu.VMEM((2, TOK), F32),
             pltpu.VMEM((4, D, FS), F32),
             pltpu.VMEM((2, FS, D), F32),
-            dma((7,)),
-            dma((7,)),
+            dma((8,)),
+            dma((8,)),
         ],
         compiler_params=pltpu.CompilerParams(vmem_limit_bytes=63 * 1024 * 1024),
     )(tg, gg, dg, du, dd)

time: 122 us -> 114 us (0.934)
  Pallas kernels: 121 us -> 112 us
    pallas_call x1, Pallas kernels: 117 us -> 109 us  [shards(): pl.pallas_call(kernel, out_shape=(jax.ShapeDtypeStruct((TOK, D), BF16), j...]
    pallas_call x1, Pallas kernels: 4.27 us -> 3.05 us  [shards(): pl.pallas_call(carry, out_shape=(jax.ShapeDtypeStruct((TOK, D), BF16), ja...]
where the time goes in v2:
time: 114 us; the launch traced here: 113 us
  Pallas kernels  112 us (98%)
    pallas_call x1, Pallas kernels, shards(): pl.pallas_call(kernel, out_shape=(jax.ShapeDtypeStruct((TOK, D), BF16), j...  109 us
    pallas_call x1, Pallas kernels, shards(): pl.pallas_call(carry, out_shape=(jax.ShapeDtypeStruct((TOK, D), BF16), ja...  3.05 us

profile of v2, /device:TPU:10, one launch (start us, length us, event | category | flops | bytes accessed | tf_op | source)
XLA Modules:
  0.0 113.2 jit_solution(5354102911231977363)
XLA Ops:
  0.6 109.4 %shard_map.110 = (bf16[256,1024]{1,0:T(8,128)(2,1)}, f32[2,256]{1,0:T(2,128)}, f32[2,1024,128]{2,1,0:T(8,128)}, f32[2,1024,128]{2,1,0:T(8,128)}, f32[2,128,1024]{2,1,0:T(8,128)}) custom-call(bf16[256,1024]{1,0:T(8,128)(2,1)} %tok.1, bf16[256,1024]{1,0:T(8,128)(2,1)} %cot.1, s32[2,256]{1,0:T(2,128)} %bitcast.3, f32[2,256]{1,0:T(2,128)} %bitcast.4, ...), custom_call_target="tpu_custom_call" | custom-call | tf_op jit(solution)/shard_map/pallas_call | solution.py:664
  110.0 3.0 %shard_map.111 = (bf16[256,1024]{1,0:T(8,128)(2,1)}, f32[2,256]{1,0:T(2,128)}, f32[2,1024,128]{2,1,0:T(8,128)}, f32[2,1024,128]{2,1,0:T(8,128)}, f32[2,128,1024]{2,1,0:T(8,128)}) custom-call(bf16[256,1024]{1,0:T(8,128)(2,1)} %get-tuple-element.15.tg, f32[2,256]{1,0:T(2,128)} %get-tuple-element.16.gg, f32[2,1024,128]{2,1,0:T(8,128)} %get-tuple-element.17.dg, ...), custom_call_target="tpu_custom_call" | custom-call | tf_op jit(solution)/shard_map/pallas_call | solution.py:681

commit v3 on v2

--- a/solution.py
+++ b/solution.py
@@ -126,32 +126,38 @@
     def toward(dz, plus):
         return (dz + 1, at_z(1)) if plus else ((dz + NZ - 1) % NZ, at_z(NZ - 1))
 
-    def z_push(dz, k, plus):
+    count = {"z": 0, "x": 0}
+
+    def z_push(dz, k, plus, a):
         to, dev = toward(dz, plus)
-        src, i = bk.at[HELD[dz, k]], HELD[to, k]
-        if to == 4:
-            a = 0 if plus else 1
-            push(src.at[a], bk.at[i, a], z_s, z_r.at[i + a], dev)
-        else:
-            push(src, bk.at[i], z_s, z_r.at[i], dev)
+        i = HELD[to, k]
+        count["z"] += 1
+        push(bk.at[HELD[dz, k], a], bk.at[i, a], z_s, z_r.at[i, a], dev)
+
+    def z_own(k):
+        for step in range(2):
+            z_push(0, k, True, step)
+            z_push(0, k, False, 1 - step)
 
     @jax.named_scope("z_take")
-    def z_take(dz, k, onward=True):
-        i = HELD[dz, k]
-        plus = dz < 4
-        first = k == 0
-        if first:
-            done(rb.at[dz], rb_r.at[dz])
-            if dz < 4 or dz > 5:
-                if dz != 4:
-                    rb_push(dz, plus)
-        if dz == 4:
-            for a in range(2):
-                done(bk.at[i, a], z_r.at[i + a])
-            return
-        done(bk.at[i], z_r.at[i])
-        if k in BRINGS[toward(dz, plus)[0]]:
-            z_push(dz, k, plus)
+    def z_take(dz, k, step):
+        for near in (dz, NZ - dz):
+            plus = near < 4 or (dz == 4 and step == 0)
+            a = step if near < 4 else 1 - step
+            if dz == 4:
+                a = step
+            i = HELD[near, k]
+            if k == 0 and step == 0:
+                if dz < 4:
+                    done(rb.at[near], rb_r.at[near])
+                    if near != 5:
+                        rb_push(near, plus)
+            done(bk.at[i, a], z_r.at[i, a])
+            if dz == 4:
+                return
+            to = toward(near, plus)[0]
+            if k in BRINGS[to] and (to != 4 or step == 0):
+                z_push(near, k, plus, a)
 
     def rb_push(dz, plus):
         if plus:
@@ -212,6 +218,7 @@
     def x_push(dz):
         pos = POS[dz]
         landed(dz, 0)
+        count["x"] += (1 not in BRINGS[dz]) + (2 not in BRINGS[dz])
         if 1 not in BRINGS[dz]:
             push(rq.at[0, pos], rq.at[1, pos], x_s, x_r.at[0, pos], at_x(1))
         if 2 not in BRINGS[dz]:
@@ -234,8 +241,9 @@
     def compute_wait(*blocks):
         for dz in blocks:
             pos, own = POS[dz], BRINGS[dz]
-            for k in own[1:]:
-                landed(dz, k)
+            for k in own:
+                if k:
+                    landed(dz, k)
             if 3 not in own:
                 done(rq.at[3, pos, low], xf_r.at[0])
                 done(rq.at[3, pos, high], xf_r.at[1])
@@ -421,9 +429,9 @@
         ig_wait(dz)
         input_grad(dz)
 
-    for plus in (True, False):
-        z_push(0, 0, plus)
-        rb_push(0, plus)
+    rb_push(0, True)
+    rb_push(0, False)
+    z_own(0)
     slots_of(0)
     done(bk.at[pl.ds(0, 2)], in_s.at[3])
     done(wv, in_s.at[4])
@@ -439,59 +447,67 @@
             push(wgu.at[(x + s) % NX], wq.at[s - 1], w_s, w_r, at_x(s))
         done(wds, in_s.at[5])
 
-    def take(blocks, k):
-        for dz in blocks:
-            z_take(dz, k)
-
     def make(blocks, k):
         for dz in blocks:
             if k == 0:
                 slots_of(dz)
             build(dz, k)
 
-    take((1, 7), 0)
+    z_take(1, 0, 0)
+    z_take(1, 0, 1)
     make((1, 7), 0)
     x_push(0)
-    take((2, 6), 0)
-    z_push(0, 3, True)
-    z_push(0, 3, False)
+    z_take(2, 0, 0)
+    z_take(2, 0, 1)
     make((2, 6), 0)
     x_push(1)
     x_push(7)
+    z_take(3, 0, 0)
+    z_own(3)
+    x_push(2)
+    z_take(3, 0, 1)
+    make((3, 5), 0)
+    x_push(6)
+    z_take(1, 3, 0)
+    with jax.named_scope("z_take"):
+        done(rb.at[4], rb_r.at[4])
+        z_take(4, 0, 0)
+        z_take(4, 0, 1)
+    make((4,), 0)
+    z_take(1, 3, 1)
+    make((1, 7), 3)
     compute_wait(0)
     compute(0)
-    x_push(2)
-    x_push(6)
-    take((3, 5), 0)
-    make((3, 5), 0)
-    take((1, 7), 3)
-    make((1, 7), 3)
     x_push(3)
     x_push(5)
-    take((4,), 0)
-    make((4,), 0)
     x_push(4)
-    take((2, 6), 3)
+    z_take(2, 3, 0)
+    z_take(2, 3, 1)
     make((2, 6), 3)
-    z_push(0, 2, True)
-    z_push(0, 1, False)
+    z_take(3, 3, 0)
+    for step in range(2):
+        z_push(0, 2, True, step)
+        z_push(0, 1, False, 1 - step)
+    z_take(3, 3, 1)
+    make((3, 5), 3)
     compute_wait(2, 6)
     compute(2, 6)
+    g_push(2)
     x_pass(4)
-    g_push(2)
     g_push(6)
-    take((3, 5), 3)
-    make((3, 5), 3)
-    z_take(1, 2)
-    z_take(7, 1)
+    compute_wait(3, 5)
+    compute(3, 5)
+    with jax.named_scope("z_extra"):
+        done(bk.at[HELD[1, 2], 0], z_r.at[HELD[1, 2], 0])
+        done(bk.at[HELD[1, 2], 1], z_r.at[HELD[1, 2], 1])
+        done(bk.at[HELD[7, 1], 0], z_r.at[HELD[7, 1], 0])
+        done(bk.at[HELD[7, 1], 1], z_r.at[HELD[7, 1], 1])
     build(1, 2)
     build(7, 1)
     g_pass(2)
     compute_wait(4)
     compute(4)
     g_push(4)
-    compute_wait(3, 5)
-    compute(3, 5)
     g_pass(6)
     g_push(3)
     with jax.named_scope("wq_wait"):
@@ -502,12 +518,12 @@
     grad(6)
     compute_wait(1, 7)
     compute(1, 7)
-
-    for s in range(1, NX):
-        push(pr, prx.at[s - 1], p_s, p_r, at_x(s))
     g_pass(3)
     g_push(1)
     grad(4)
+
+    for s in range(1, NX):
+        push(pr, prx.at[s - 1], p_s, p_r, at_x(s))
     g_pass(5)
     g_push(7)
     dense(2)
@@ -578,10 +594,10 @@
     with jax.named_scope("gather"):
         done(gx.at[0, pl.ds(0, 3 * TOK)], t_r)
     with jax.named_scope("drain"):
-        done(bk.at[pl.ds(0, 15)], z_s)
+        done(bk.at[pl.ds(0, count["z"] // 2)], z_s)
         done(rb.at[pl.ds(0, 7)], rb_s)
         done(sx.at[:, pl.ds(1, PLANE - 1)], ip_s)
-        done(rq.at[pl.ds(0, 2), pl.ds(0, 7)], x_s)
+        done(rq.at[pl.ds(0, 2), pl.ds(0, count["x"] // 2)], x_s)
         done(rq.at[0, 0], xf_s)
         done(wq, w_s)
         done(gx.at[pl.ds(0, 2)], g_s)
@@ -654,7 +670,7 @@
         pltpu.VMEM((2, D, FS), F32),
         pltpu.VMEM((2, D, FS), F32),
         pltpu.VMEM((2, FS, D), F32),
-        dma((6,)), dma, dma((len(HELD) + 1,)), dma, dma((8,)),
+        dma((6,)), dma, dma((len(HELD), 2)), dma, dma((8,)),
         dma, dma((len(BUILT),)),
         dma, dma((2, 8)), dma, dma((2,)),
         dma, dma, dma, dma((2, 8)), dma, dma((2, 8)),

time: 114 us -> 111 us (0.974); the launches traced: 113 us -> 109 us
  Pallas kernels: 112 us -> 108 us
    pallas_call x1, Pallas kernels: 109 us -> 105 us  [shards(): pl.pallas_call(kernel, out_shape=(jax.ShapeDtypeStruct((TOK, D), BF16), j...]
where the time goes in v3:
time: 111 us; the launch traced here: 109 us
  Pallas kernels  108 us (97%)
    pallas_call x1, Pallas kernels, shards(): pl.pallas_call(kernel, out_shape=(jax.ShapeDtypeStruct((TOK, D), BF16), j...  105 us
    pallas_call x1, Pallas kernels, shards(): pl.pallas_call(carry, out_shape=(jax.ShapeDtypeStruct((TOK, D), BF16), ja...  3.05 us

profile of v3, /device:TPU:10, one launch (start us, length us, event | category | flops | bytes accessed | tf_op | source)
XLA Modules:
  0.0 109.0 jit_solution(525679980124717384)
XLA Ops:
  0.6 105.2 %shard_map.110 = (bf16[256,1024]{1,0:T(8,128)(2,1)}, f32[2,256]{1,0:T(2,128)}, f32[2,1024,128]{2,1,0:T(8,128)}, f32[2,1024,128]{2,1,0:T(8,128)}, f32[2,128,1024]{2,1,0:T(8,128)}) custom-call(bf16[256,1024]{1,0:T(8,128)(2,1)} %tok.1, bf16[256,1024]{1,0:T(8,128)(2,1)} %cot.1, s32[2,256]{1,0:T(2,128)} %bitcast.3, f32[2,256]{1,0:T(2,128)} %bitcast.4, ...), custom_call_target="tpu_custom_call" | custom-call | tf_op jit(solution)/shard_map/pallas_call | solution.py:680
  105.8 3.0 %shard_map.111 = (bf16[256,1024]{1,0:T(8,128)(2,1)}, f32[2,256]{1,0:T(2,128)}, f32[2,1024,128]{2,1,0:T(8,128)}, f32[2,1024,128]{2,1,0:T(8,128)}, f32[2,128,1024]{2,1,0:T(8,128)}) custom-call(bf16[256,1024]{1,0:T(8,128)(2,1)} %get-tuple-element.15.tg, f32[2,256]{1,0:T(2,128)} %get-tuple-element.16.gg, f32[2,1024,128]{2,1,0:T(8,128)} %get-tuple-element.17.dg, ...), custom_call_target="tpu_custom_call" | custom-call | tf_op jit(solution)/shard_map/pallas_call | solution.py:697

commit v4 on v3

--- a/solution.py
+++ b/solution.py
@@ -318,14 +318,13 @@
     def g_pass(dz):
         lo, hi = rows_of(dz, 0, 96), rows_of(dz, 96, 96)
         done(gx.at[1, rows_of(dz)], g_r.at[0, dz])
-        push(gx.at[1, lo], gx.at[3, lo], gf_s, gf_r.at[0, dz], at_x(1))
+        push(gx.at[1, lo], gx.at[3, lo], gf_s, gf_r.at[dz], at_x(1))
         done(gx.at[2, rows_of(dz)], g_r.at[1, dz])
-        push(gx.at[2, hi], gx.at[3, hi], gf_s, gf_r.at[1, dz], at_x(NX - 1))
+        push(gx.at[2, hi], gx.at[3, hi], gf_s, gf_r.at[dz], at_x(NX - 1))
 
     @jax.named_scope("ig_wait")
     def ig_wait(dz):
-        done(gx.at[3, rows_of(dz, 0, 96)], gf_r.at[0, dz])
-        done(gx.at[3, rows_of(dz, 96, 96)], gf_r.at[1, dz])
+        done(gx.at[3, rows_of(dz)], gf_r.at[dz])
 
     @jax.named_scope("input_grad")
     def input_grad(dz):
@@ -529,29 +528,29 @@
     dense(2)
     dense(6)
     grad(3)
-    products()
     g_pass(1)
     g_push(0)
     dense(4)
     for i in range(4):
         chain(4, i)
+    products()
     grad(5)
     dense(3)
     early(3)
     g_pass(7)
     later(3)
-    grad(1)
     dense(5)
     early(5)
+    grad(1)
+    early(2)
     later(5)
     g_pass(0)
-    early(2)
     grad(7)
     later(2)
     early(6)
     dense(1)
+    later(6)
     early(1)
-    later(6)
     grad(0)
     later(1)
     dense(7)
@@ -673,7 +672,7 @@
         dma((6,)), dma, dma((len(HELD), 2)), dma, dma((8,)),
         dma, dma((len(BUILT),)),
         dma, dma((2, 8)), dma, dma((2,)),
-        dma, dma, dma, dma((2, 8)), dma, dma((2, 8)),
+        dma, dma, dma, dma((2, 8)), dma, dma((8,)),
         dma, dma, dma, dma, dma, dma, dma, dma((8,)),
         dma, dma((4, 8)), dma, dma, dma((5,)),
     ]

time: 111 us -> 110 us (level)
  no operation moved by 1% of the time
where the time goes in v4:
time: 110 us; the launch traced here: 109 us
  Pallas kernels  108 us (98%)
    pallas_call x1, Pallas kernels, shards(): pl.pallas_call(kernel, out_shape=(jax.ShapeDtypeStruct((TOK, D), BF16), j...  105 us
    pallas_call x1, Pallas kernels, shards(): pl.pallas_call(carry, out_shape=(jax.ShapeDtypeStruct((TOK, D), BF16), ja...  3.05 us

profile of v4, /device:TPU:10, one launch (start us, length us, event | category | flops | bytes accessed | tf_op | source)
XLA Modules:
  0.0 109.0 jit_solution(5967355995898998201)
XLA Ops:
  0.6 105.2 %shard_map.110 = (bf16[256,1024]{1,0:T(8,128)(2,1)}, f32[2,256]{1,0:T(2,128)}, f32[2,1024,128]{2,1,0:T(8,128)}, f32[2,1024,128]{2,1,0:T(8,128)}, f32[2,128,1024]{2,1,0:T(8,128)}) custom-call(bf16[256,1024]{1,0:T(8,128)(2,1)} %tok.1, bf16[256,1024]{1,0:T(8,128)(2,1)} %cot.1, s32[2,256]{1,0:T(2,128)} %bitcast.3, f32[2,256]{1,0:T(2,128)} %bitcast.4, ...), custom_call_target="tpu_custom_call" | custom-call | tf_op jit(solution)/shard_map/pallas_call | solution.py:679
  105.8 3.0 %shard_map.111 = (bf16[256,1024]{1,0:T(8,128)(2,1)}, f32[2,256]{1,0:T(2,128)}, f32[2,1024,128]{2,1,0:T(8,128)}, f32[2,1024,128]{2,1,0:T(8,128)}, f32[2,128,1024]{2,1,0:T(8,128)}) custom-call(bf16[256,1024]{1,0:T(8,128)(2,1)} %get-tuple-element.15.tg, f32[2,256]{1,0:T(2,128)} %get-tuple-element.16.gg, f32[2,1024,128]{2,1,0:T(8,128)} %get-tuple-element.17.dg, ...), custom_call_target="tpu_custom_call" | custom-call | tf_op jit(solution)/shard_map/pallas_call | solution.py:696
